TPU v7x, 256 devices: a whole 4x4x8 slice. The times are simulated.
256 devices in a mesh: ep: 32 (over z, x), tp: 8 (over y, core).
Axes of the slice: x: 4, y: 4, z: 8, core: 2. Of those that a mesh axis runs over, the one named last changes fastest.
Arguments:
- queries: bfloat16 [4096, 4096], P('ep', 'tp'), may hold values from -6 to 6
- key_rows: bfloat16 [4096, 4096], P('ep', 'tp'), may hold values from -6 to 6
- value_rows: bfloat16 [4096, 4096], P('ep', 'tp'), may hold values from -6 to 6
- key_shift: bfloat16 [4096, 64], P('ep', 'tp'), may hold values from -20 to 1
- out_weight: bfloat16 [4096, 4096], P('tp'), may hold values from -0.09375 to 0.09375
- routed_rows: bfloat16 [4096, 4096], P('ep'), may hold values from -6 to 6
- expert_ids: int32 [4096, 2], P('ep'), may hold values from 0 to 31, as said below
- route_weights: float32 [4096, 2], P(('ep', 'tp')), may hold values from 0.2 to 1
- gate_weight: bfloat16 [32, 4096, 1024], P('ep', None, 'tp'), may hold values from -0.09375 to 0.09375
- up_weight: bfloat16 [32, 4096, 1024], P('ep', None, 'tp'), may hold values from -0.09375 to 0.09375
- down_weight: bfloat16 [32, 1024, 4096], P('ep', 'tp'), may hold values from -0.1875 to 0.1875
Outputs:
- mixed_rows: bfloat16 [4096, 4096], P(('ep', 'tp'))
- routed_out: bfloat16 [4096, 4096], P(('ep', 'tp'))
Inputs may be any that keep to these rules, and one draw needn't show every extreme that they name: `expert_ids`: the two ids of a token differ and lie in one group of 8 consecutive experts. Within each aligned block of 16 tokens no expert is named more than 2 times.
All inputs are finite; a program needn't handle non-finite values.
Results may differ from a plain program's by a relative error of at most 0.015.
Values may be sent and summed in bfloat16 or wider, within the bound.
No kernel may reach another device: no remote copies, remote signals or barrier semaphores. Data moves between devices by JAX's collectives and lax.ppermute only.
A program may use at most 128 MiB of HBM per device.

v0:
```python
import jax
import jax.numpy as jnp
from jax import lax
from jax.experimental import pallas as pl
from jax.experimental.pallas import tpu as pltpu
from jax.sharding import Mesh, PartitionSpec as P


HEAD = 64
Z, X, Y, C = 8, 4, 4, 2
BF = jnp.bfloat16
F32 = jnp.float32

STEPS = (
    ((7, 6), (6, 5), (5, 4), (4, 3)),
    ((7, 5), (6, 4), (5, 3), (4, 2)),
    ((7, 4), (6, 3), (5, 2), (4, 1)),
    ((7, 3), (6, 2), (5, 1), (4, 0)),
    ((7, 2), (6, 1), (5, 0), (3, 2)),
    ((7, 1), (6, 0), (3, 1), (2, 1)),
    ((7, 0), (3, 0), (2, 0), (1, 0)),
)


def attend_kernel(*refs):
    arrived, (k1_ref, k2_ref, k3_ref, o_ref) = refs[:Z], refs[Z : Z + 4]
    attend_body(arrived, k1_ref, k2_ref, k3_ref, o_ref, *refs[Z + 4 :])


def attend_body(arrived, k1_ref, k2_ref, k3_ref, o_ref, kv_ref, qs_ref, tri_ref, carry_ref, acc_ref, steps_ref):
    here = lax.axis_index("x")
    plane = lax.axis_index("z")
    for i in range(Z):
        at = lax.rem(plane + (Z - i), Z)
        kv_ref[here, at] = arrived[i][HEAD:]
        for shift, piece in ((1, k1_ref), (2, k2_ref), (3, k3_ref)):
            kv_ref[lax.rem(here + (X - shift), X), at] = piece[i]
    row = lax.broadcasted_iota(jnp.int32, (256, 256), 0)
    col = lax.broadcasted_iota(jnp.int32, (256, 256), 1)
    tri = jnp.where(row > col, 1.0, 0.0).astype(BF)
    tri_ref[0:256] = tri
    tri_ref[256:512] = tri
    ones = jnp.where(lax.broadcasted_iota(jnp.int32, (64, 128), 0) == 0, 1.0, 0.0)
    for i in range(Z):
        q = jnp.concatenate([arrived[i][:HEAD].astype(F32), ones], axis=0)
        qs_ref[lax.rem(plane + (Z - i), Z)] = jnp.transpose(q).astype(BF)
    for i, step in enumerate(STEPS):
        for j, pair in enumerate(step):
            steps_ref[i, 2 * j] = pair[0]
            steps_ref[i, 2 * j + 1] = pair[1]

    def scores(b, t):
        keys = jnp.concatenate([kv_ref[i, t, 0:80, :] for i in range(4)], axis=1)
        return jnp.dot(qs_ref[b][:, 0:80], keys, preferred_element_type=F32)

    def tile(b, t, mask, carry):
        s = scores(b, t)
        sp = jnp.maximum(s, jnp.log(1.0 + jnp.exp(jnp.minimum(s, 80.0))))
        if mask is not None:
            sp = jnp.where(mask, sp, 0.0)
        high = sp.astype(BF)
        low = (sp - high.astype(F32)).astype(BF)
        logit = s - sp
        weights = [None, None]
        for half in (1, 0):
            at = slice(half * 256, half * 256 + 256)
            after = jnp.dot(
                jnp.concatenate([high[:, at], low[:, at]], axis=1), tri_ref[...], preferred_element_type=F32
            )
            w = jnp.exp(logit[:, at] - after - carry)
            if mask is not None:
                w = jnp.where(mask[:, at], w, 0.0)
            weights[half] = w.astype(BF)
            carry = carry + after[:, 0:1] + sp[:, half * 256 : half * 256 + 1]
        values = jnp.concatenate([kv_ref[i, t, 80:144, :] for i in range(4)], axis=1)
        out = lax.dot_general(
            jnp.concatenate(weights, axis=1), values, (((1,), (1,)), ((), ())), preferred_element_type=F32
        )
        return out, carry

    def diagonal(i, unused):
        q_at = here * 128 + lax.broadcasted_iota(jnp.int32, (128, 512), 0)
        mask = lax.broadcasted_iota(jnp.int32, (128, 512), 1) < q_at
        done = [tile(i * 4 + j, i * 4 + j, mask, jnp.zeros((128, 1), F32)) for j in range(4)]
        for j in range(4):
            acc_ref[i * 4 + j] = done[j][0]
            carry_ref[i * 4 + j] = done[j][1]
        return unused

    lax.fori_loop(0, 2, diagonal, 0)

    def sweep(i, unused):
        blocks = [steps_ref[i, 2 * j] for j in range(4)]
        tiles = [steps_ref[i, 2 * j + 1] for j in range(4)]
        carries = [carry_ref[b] for b in blocks]
        before = [acc_ref[b] for b in blocks]
        done = [tile(blocks[j], tiles[j], None, carries[j]) for j in range(4)]
        for j in range(4):
            acc_ref[blocks[j]] = before[j] + done[j][0]
            carry_ref[blocks[j]] = done[j][1]
        return unused

    lax.fori_loop(0, len(STEPS), sweep, 0)
    for b in range(8):
        o_ref[b] = jnp.transpose(acc_ref[b]).astype(BF)


VMEM = pl.BlockSpec(memory_space=pltpu.VMEM)
ANY = pl.BlockSpec(memory_space=pl.ANY)


def attend(arrived, pieces):
    return pl.pallas_call(
        attend_kernel,
        out_shape=jax.ShapeDtypeStruct((8, HEAD, 128), BF),
        in_specs=[VMEM] * (Z + 3),
        out_specs=VMEM,
        scratch_shapes=[
            pltpu.VMEM((4, 8, 144, 128), BF),
            pltpu.VMEM((8, 128, 128), BF),
            pltpu.VMEM((512, 256), BF),
            pltpu.VMEM((8, 128, 1), F32),
            pltpu.VMEM((8, 128, HEAD), F32),
            pltpu.SMEM((len(STEPS), 8), jnp.int32),
        ],
        compiler_params=pltpu.CompilerParams(vmem_limit_bytes=32 * 1024 * 1024),
        cost_estimate=pl.CostEstimate(flops=4_000_000_000, transcendentals=7_000_000, bytes_accessed=2_000_000),
    )(*arrived, *pieces)


def pack_kernel(q_ref, k_ref, v_ref, shift_ref, *refs):
    outs, (q_all, k_all, v_all, shift_all) = refs[:Z], refs[Z:]
    plane = lax.axis_index("z")
    q_all[...] = jnp.transpose(q_ref[...].astype(F32) * HEAD**-0.5)
    k_all[...] = jnp.transpose(k_ref[...].astype(F32))
    v_all[...] = jnp.transpose(v_ref[...].astype(F32))
    shift_all[...] = shift_ref[...].astype(F32)
    first = lax.broadcasted_iota(jnp.int32, (16, 128), 0) == 0
    for s, out in enumerate(outs):
        head = lax.rem(plane + s, Z)
        rows = pl.ds(pl.multiple_of(head * HEAD, HEAD), HEAD)
        out[0:64] = q_all[rows, :].astype(BF)
        out[64:128] = k_all[rows, :].astype(BF)
        shift = jnp.broadcast_to(shift_all[pl.ds(head, 1), :], (16, 128))
        out[128:144] = jnp.where(first, shift, 0.0).astype(BF)
        out[144:208] = v_all[rows, :].astype(BF)


def stack_kernel(*refs):
    for i in range(Z):
        refs[Z][i] = refs[i][HEAD:]


def stacked(arrived):
    return pl.pallas_call(
        stack_kernel,
        out_shape=jax.ShapeDtypeStruct((Z, 144, 128), BF),
        in_specs=[VMEM] * Z,
        out_specs=VMEM,
    )(*arrived)


def pack(queries, key_rows, value_rows, shift):
    rows, width = queries.shape
    return pl.pallas_call(
        pack_kernel,
        out_shape=[jax.ShapeDtypeStruct((208, 128), BF)] * Z,
        in_specs=[VMEM] * 4,
        out_specs=[VMEM] * Z,
        scratch_shapes=[pltpu.VMEM((width, rows), F32)] * 3 + [pltpu.VMEM((8, rows), F32)],
    )(queries, key_rows, value_rows, shift)


def shifted(value, axis, size, by):
    return lax.ppermute(value, axis, [(i, (i + by) % size) for i in range(size)])


def mixer(queries, key_rows, value_rows, key_shift, out_weight):
    heads = key_shift.shape[1]
    rows = queries.shape[0]
    packed = pack(queries, key_rows, value_rows, key_shift.T)
    arrived = [packed[0]] + [shifted(packed[by], "z", Z, by) for by in range(1, Z)]
    keys = stacked(arrived)
    pieces = [shifted(keys, "x", X, by) for by in (1, 2, 3)]
    out = attend(arrived, pieces)
    attended = lax.all_to_all(out, "z", split_axis=0, concat_axis=0, tiled=True)
    attended = attended.reshape(heads * HEAD, rows)
    partial = lax.dot_general(
        attended, out_weight, (((0,), (0,)), ((), ())), preferred_element_type=F32
    ).astype(BF)
    return summed_over_tp(partial)


def summed_over_tp(partial):
    y, core = lax.axis_index("y"), lax.axis_index("c")
    rows, width = partial.shape
    per = rows // (Y * C)
    parts = partial.reshape(Y, C, per, width)
    mine = lax.dynamic_index_in_dim(parts, core, 1, keepdims=False)
    other = lax.dynamic_index_in_dim(parts, 1 - core, 1, keepdims=False)
    both = (mine.astype(F32) + shifted(other, "c", C, 1).astype(F32)).astype(BF)
    total = lax.dynamic_index_in_dim(both, y, 0, keepdims=False).astype(F32)
    for by in (1, 2, 3):
        piece = lax.dynamic_index_in_dim(both, lax.rem(y + by, Y), 0, keepdims=False)
        total = total + shifted(piece, "y", Y, by).astype(F32)
    return total.astype(BF)


def selection(ids_ref, core):
    row = lax.broadcasted_iota(jnp.int32, (256, 128), 0)
    token = lax.broadcasted_iota(jnp.int32, (256, 128), 1)
    expert = lax.div(row, 8)
    named = [ids_ref[k : k + 1, :] == expert for k in range(2)]
    either = jnp.where(named[0] | named[1], 1.0, 0.0)
    before = lax.broadcasted_iota(jnp.int32, (128, 128), 0)
    after = lax.broadcasted_iota(jnp.int32, (128, 128), 1)
    earlier = jnp.where((before < after) & (lax.div(before, 16) == lax.div(after, 16)), 1.0, 0.0)
    slot = jnp.dot(either.astype(BF), earlier.astype(BF), preferred_element_type=F32)
    here = (lax.div(token, 16) == 2 * lax.div(lax.rem(row, 8), 2) + core) & (
        slot == lax.rem(row, 2).astype(F32)
    )
    return [jnp.where(n & here, 1.0, 0.0) for n in named]


def dispatch_kernel(ids_ref, rows_ref, out_ref, part_ref, sem):
    width = out_ref.shape[1]
    start = pl.multiple_of(lax.axis_index("y") * width, width)
    copy = pltpu.make_async_copy(rows_ref.at[:, pl.ds(start, width)], part_ref, sem)
    copy.start()
    first, second = selection(ids_ref, lax.axis_index("c"))
    pick = (first + second).astype(BF)
    copy.wait()
    out_ref[...] = jnp.dot(pick, part_ref[...], preferred_element_type=F32).astype(BF)


def dispatch(ids, rows):
    width = rows.shape[1] // Y
    return pl.pallas_call(
        dispatch_kernel,
        out_shape=jax.ShapeDtypeStruct((256, width), BF),
        in_specs=[VMEM, ANY],
        out_specs=VMEM,
        scratch_shapes=[pltpu.VMEM((128, width), BF), pltpu.SemaphoreType.DMA],
    )(ids, rows)


def collect_kernel(ids_ref, rows_ref, o0_ref, o1_ref, o2_ref, o3_ref, all_ref):
    y, core = lax.axis_index("y"), lax.axis_index("c")
    for k, pick in enumerate(selection(ids_ref, core)):
        chosen = jnp.transpose(pick).astype(BF)
        all_ref[k] = jnp.dot(chosen, rows_ref[...], preferred_element_type=F32).astype(BF)
        for s, out in enumerate((o0_ref, o1_ref, o2_ref, o3_ref)):
            at = pl.multiple_of((2 * lax.rem(y + s, Y) + core) * 16, 16)
            out[k] = all_ref[k, pl.ds(at, 16), :]


def collect(ids, rows):
    width = rows.shape[1]
    return pl.pallas_call(
        collect_kernel,
        out_shape=[jax.ShapeDtypeStruct((2, 16, width), BF)] * Y,
        in_specs=[VMEM, VMEM],
        out_specs=[VMEM] * Y,
        scratch_shapes=[pltpu.VMEM((2, 128, width), BF)],
    )(ids, rows)


def finish_kernel(p0_ref, p1_ref, p2_ref, p3_ref, weights_ref, out_ref):
    w = weights_ref[...]
    width = p0_ref.shape[2]
    for s, p in enumerate((p0_ref, p1_ref, p2_ref, p3_ref)):
        at = pl.multiple_of(lax.rem(lax.axis_index("y") + (Y - s), Y) * width, width)
        total = p[0].astype(F32) * w[:, 0:1] + p[1].astype(F32) * w[:, 1:2]
        out_ref[:, pl.ds(at, width)] = total.astype(BF)


def finish(picked, weights):
    return pl.pallas_call(
        finish_kernel,
        out_shape=jax.ShapeDtypeStruct((16, Y * picked[0].shape[2]), BF),
        in_specs=[VMEM] * 5,
        out_specs=VMEM,
    )(*picked, weights)


def share_kernel(gate_ref, up_ref, down_ref, o1_ref, o2_ref, o3_ref, sem):
    width = gate_ref.shape[0] // Y
    copies = []
    for s, out in ((1, o1_ref), (2, o2_ref), (3, o3_ref)):
        start = pl.multiple_of(lax.rem(lax.axis_index("y") + s, Y) * width, width)
        copies.append((gate_ref.at[pl.ds(start, width), :], out.at[pl.ds(0, width), :]))
        copies.append((up_ref.at[pl.ds(start, width), :], out.at[pl.ds(width, width), :]))
        for j in range(width // 128):
            copies.append(
                (
                    down_ref.at[:, pl.ds(pl.multiple_of(start + j * 128, 128), 128)],
                    out.at[pl.ds(2 * width + j * 128, 128), :],
                )
            )
    made = [pltpu.make_async_copy(a, b, sem.at[n]) for n, (a, b) in enumerate(copies)]
    for m in made:
        m.start()
    for m in made:
        m.wait()


def share(gate, up, down):
    width = gate.shape[0] // Y
    out = jax.ShapeDtypeStruct((3 * width, 128), BF)
    return pl.pallas_call(
        share_kernel,
        out_shape=[out] * (Y - 1),
        in_specs=[ANY, ANY, ANY],
        out_specs=[VMEM] * (Y - 1),
        scratch_shapes=[pltpu.SemaphoreType.DMA(((Y - 1) * (2 + width // 128),))],
    )(gate, up, down)


def expand_kernel(
    own_ref, other_ref, gate_ref, up_ref, w1_ref, w2_ref, w3_ref, o0_ref, o1_ref, o2_ref, o3_ref, kept_ref, sem
):
    width = own_ref.shape[1]
    rows = own_ref.shape[0]
    start = pl.multiple_of(lax.axis_index("y") * width, width)
    copies = [
        pltpu.make_async_copy(ref.at[pl.ds(start, width), :], kept_ref.at[n], sem.at[n])
        for n, ref in enumerate((gate_ref, up_ref))
    ]
    for copy in copies:
        copy.start()

    def into(o_ref, w):
        o_ref[0:rows] = jnp.dot(own_ref[...], w, preferred_element_type=F32).astype(o_ref.dtype)
        o_ref[rows : 2 * rows] = jnp.dot(other_ref[...], w, preferred_element_type=F32).astype(o_ref.dtype)

    for w_ref, o_ref in ((w1_ref, o1_ref), (w2_ref, o2_ref), (w3_ref, o3_ref)):
        into(o_ref, jnp.concatenate([w_ref[0:width], w_ref[width : 2 * width]], axis=1))
    for copy in copies:
        copy.wait()
    into(o0_ref, jnp.concatenate([kept_ref[0], kept_ref[1]], axis=1))


def expand(own, other, gate, up, shared):
    rows = 2 * own.shape[0]
    width = own.shape[1]
    sent = jax.ShapeDtypeStruct((rows, 256), BF)
    return pl.pallas_call(
        expand_kernel,
        out_shape=[jax.ShapeDtypeStruct((rows, 256), F32), sent, sent, sent],
        in_specs=[VMEM, VMEM, ANY, ANY] + [VMEM] * 3,
        out_specs=[VMEM] * 4,
        scratch_shapes=[pltpu.VMEM((2, width, 128), BF), pltpu.SemaphoreType.DMA((2,))],
        compiler_params=pltpu.CompilerParams(vmem_limit_bytes=32 * 1024 * 1024),
    )(own, other, gate, up, *shared)


def hidden_kernel(p0_ref, p1_ref, p2_ref, p3_ref, o_ref):
    both = p0_ref[...]
    for p in (p1_ref, p2_ref, p3_ref):
        both = both + p[...].astype(F32)
    gate, up = both[:, 0:128], both[:, 128:256]
    o_ref[...] = (gate / (1.0 + jnp.exp(-gate)) * up).astype(BF)


def hidden_units(parts):
    return pl.pallas_call(
        hidden_kernel,
        out_shape=jax.ShapeDtypeStruct((parts[0].shape[0], 128), BF),
        in_specs=[VMEM] * 4,
        out_specs=VMEM,
    )(*parts)


def reduce_kernel(
    h0_ref, h1_ref, h2_ref, h3_ref, down_ref, w1_ref, w2_ref, w3_ref, own_ref, other_ref, kept_ref, sem
):
    rows, width = own_ref.shape
    start = pl.multiple_of(lax.axis_index("y") * width, width)
    copy = pltpu.make_async_copy(down_ref.at[:, pl.ds(start, width)], kept_ref, sem)
    copy.start()
    units = jnp.concatenate([h[...] for h in (h1_ref, h2_ref, h3_ref, h0_ref)], axis=1)
    columns = []
    for w_ref in (w1_ref, w2_ref, w3_ref):
        blocks = [w_ref[2 * width + j * 128 : 2 * width + j * 128 + 128] for j in range(width // 128)]
        columns.append(jnp.concatenate(blocks, axis=1))
    copy.wait()
    w = jnp.concatenate(columns + [kept_ref[...]], axis=0)
    other_ref[...] = jnp.dot(units[rows:], w, preferred_element_type=F32).astype(BF)
    own_ref[...] = jnp.dot(units[:rows], w, preferred_element_type=F32)


def reduce_units(units, down, shared):
    rows = units[0].shape[0] // 2
    width = shared[0].shape[0] // 3
    return pl.pallas_call(
        reduce_kernel,
        out_shape=[jax.ShapeDtypeStruct((rows, width), F32), jax.ShapeDtypeStruct((rows, width), BF)],
        in_specs=[VMEM] * 4 + [ANY] + [VMEM] * 3,
        out_specs=[VMEM] * 2,
        scratch_shapes=[pltpu.VMEM((128, width), BF), pltpu.SemaphoreType.DMA],
        compiler_params=pltpu.CompilerParams(vmem_limit_bytes=32 * 1024 * 1024),
    )(*units, down, *shared)


def add_kernel(a_ref, b_ref, o_ref):
    o_ref[...] = (a_ref[...] + b_ref[...].astype(F32)).astype(BF)


def added(a, b):
    return pl.pallas_call(
        add_kernel,
        out_shape=jax.ShapeDtypeStruct(a.shape, BF),
        in_specs=[VMEM, VMEM],
        out_specs=VMEM,
    )(a, b)


def experts(routed_rows, expert_ids, route_weights, gate_weight, up_weight, down_weight):
    ep = ("z", "x")
    ids = expert_ids.T
    width = routed_rows.shape[1] // Y
    kept = share(gate_weight[0], up_weight[0], down_weight[0])
    shared = [shifted(kept[s - 1], "y", Y, s) for s in (1, 2, 3)]
    outgoing = dispatch(ids, routed_rows).reshape(Z * X, 8, width)
    own = lax.all_to_all(outgoing, ep, split_axis=0, concat_axis=0, tiled=True).reshape(256, width)
    other = shifted(own, "c", C, 1)
    parts = expand(own, other, gate_weight[0], up_weight[0], shared)
    summed = [parts[0]] + [shifted(parts[s], "y", Y, Y - s) for s in (1, 2, 3)]
    mine = hidden_units(summed)
    units = [mine] + [shifted(mine, "y", Y, s) for s in (1, 2, 3)]
    own_out, other_out = reduce_units(units, down_weight[0], shared)
    other_out = shifted(other_out, "c", C, 1)
    result = added(own_out, other_out)
    returned = lax.all_to_all(
        result.reshape(Z * X, 8, width), ep, split_axis=0, concat_axis=0, tiled=True
    ).reshape(256, width)
    picked = collect(ids, returned)
    picked = [picked[0]] + [shifted(picked[s], "y", Y, s) for s in (1, 2, 3)]
    return finish(picked, route_weights)


def shards(
    queries,
    key_rows,
    value_rows,
    key_shift,
    out_weight,
    routed_rows,
    expert_ids,
    route_weights,
    gate_weight,
    up_weight,
    down_weight,
):
    mixed_rows = mixer(queries, key_rows, value_rows, key_shift, out_weight)
    routed_out = experts(routed_rows, expert_ids, route_weights, gate_weight, up_weight, down_weight)
    return (mixed_rows, routed_out)


def solution(mesh):
    mesh = Mesh(mesh.devices.reshape(Z, X, Y, C), ("z", "x", "y", "c"))
    ep, tp = ("z", "x"), ("y", "c")
    return jax.shard_map(
        shards,
        mesh=mesh,
        in_specs=(
            P(ep, tp),
            P(ep, tp),
            P(ep, tp),
            P(ep, tp),
            P(tp, None),
            P(ep, None),
            P(ep, None),
            P(ep + tp, None),
            P(ep, None, tp),
            P(ep, None, tp),
            P(ep, tp, None),
        ),
        out_specs=(P(ep + tp, None), P(ep + tp, None)),
        check_vma=False,
    )
```

profile of v0, /device:TPU:2, one launch (start us, length us, event | category | flops | bytes accessed | tf_op | source)
XLA Modules:
  0.0 164.3 jit_solution(10858515295792452045)
XLA Ops:
  0.7 2.9 %shard_map.125 = bf16[256,1024]{1,0:T(8,128)(2,1)} custom-call(s32[2,128]{1,0:T(2,128)} %bitcast.43, bf16[128,4096]{1,0:T(8,128)(2,1)} %rows_ref.1), custom_call_target="tpu_custom_call" | custom-call | tf_op jit(solution)/shard_map/pallas_call | solution.py:238
  3.5 11.6 %all-to-all-start.1 = ((bf16[32,8,1024]{2,1,0:T(8,128)(2,1)}), bf16[32,8,1024]{2,1,0:T(8,128)(2,1)S(1)}, u32[]{:S(2)}, u32[]{:S(2)}) async-start(bf16[32,8,1024]{2,1,0:T(8,128)(2,1)} %bitcast.40), calls=%async_computation.1 | async-start | bytes 1048576 | tf_op jit(solution)/shard_map/all_to_all | solution.py:425
  15.2 3.2 %shard_map.126 = (bf16[3072,128]{1,0:T(8,128)(2,1)}, bf16[3072,128]{1,0:T(8,128)(2,1)}, bf16[3072,128]{1,0:T(8,128)(2,1)}) custom-call(bf16[4096,128]{1,0:T(8,128)(2,1)} %bitcast.29, bf16[4096,128]{1,0:T(8,128)(2,1)} %bitcast.31, bf16[128,4096]{1,0:T(8,128)(2,1)} %bitcast.33), custom_call_target="tpu_custom_call" | custom-call | tf_op jit(solution)/shard_map/pallas_call | solution.py:310
  20.1 2.9 %collective-permute-start.16 = (bf16[3072,128]{1,0:T(8,128)(2,1)}, bf16[3072,128]{1,0:T(8,128)(2,1)}, u32[]{:S(2)}, u32[]{:S(2)}) collective-permute-start(bf16[3072,128]{1,0:T(8,128)(2,1)} %get-tuple-element.32), channel_id=1, source_target_pairs={{0,4},{2,6},{4,0},{6,2},{1,5},{3,7},{5,1},{7,3},{8,12},{10,14},{12... | collective-permute-start | bytes 2359304 | tf_op jit(solution)/shard_map/ppermute | solution.py:175
  27.8 2.4 %collective-permute-start.1 = (bf16[208,128]{1,0:T(8,128)(2,1)}, bf16[208,128]{1,0:T(8,128)(2,1)}, u32[]{:S(2)}, u32[]{:S(2)}) collective-permute-start(bf16[208,128]{1,0:T(8,128)(2,1)} %get-tuple-element.25), channel_id=1, source_target_pairs={{0,64},{32,96},{64,128},{96,160},{128,192},{160,224},{192,0},{224,... | collective-permute-start | bytes 159752 | tf_op jit(solution)/shard_map/ppermute | solution.py:175
  30.2 2.6 %collective-permute-done.refs_1_ = bf16[208,128]{1,0:T(8,128)(2,1)S(1)} collective-permute-done((bf16[208,128]{1,0:T(8,128)(2,1)}, bf16[208,128]{1,0:T(8,128)(2,1)S(1)}, u32[]{:S(2)}, u32[]{:S(2)}) %collective-permute-start) | collective-permute-done | bytes 53280 | tf_op jit(solution)/shard_map/ppermute | solution.py:175
  35.0 5.4 %collective-permute-done.2.refs_3_ = bf16[208,128]{1,0:T(8,128)(2,1)} collective-permute-done((bf16[208,128]{1,0:T(8,128)(2,1)}, bf16[208,128]{1,0:T(8,128)(2,1)}, u32[]{:S(2)}, u32[]{:S(2)}) %collective-permute-start.2) | collective-permute-done | bytes 53280 | tf_op jit(solution)/shard_map/ppermute | solution.py:175
  40.4 4.5 %collective-permute-start.3 = (bf16[208,128]{1,0:T(8,128)(2,1)}, bf16[208,128]{1,0:T(8,128)(2,1)}, u32[]{:S(2)}, u32[]{:S(2)}) collective-permute-start(bf16[208,128]{1,0:T(8,128)(2,1)} %get-tuple-element.27), channel_id=1, source_target_pairs={{0,128},{32,160},{64,192},{96,224},{128,0},{160,32},{192,64},{224,... | collective-permute-start | bytes 159752 | tf_op jit(solution)/shard_map/ppermute | solution.py:175
  44.9 3.8 %collective-permute-done.3.refs_4_ = bf16[208,128]{1,0:T(8,128)(2,1)} collective-permute-done((bf16[208,128]{1,0:T(8,128)(2,1)}, bf16[208,128]{1,0:T(8,128)(2,1)}, u32[]{:S(2)}, u32[]{:S(2)}) %collective-permute-start.3) | collective-permute-done | bytes 53280 | tf_op jit(solution)/shard_map/ppermute | solution.py:175
  48.8 3.3 %collective-permute-start.4 = (bf16[208,128]{1,0:T(8,128)(2,1)}, bf16[208,128]{1,0:T(8,128)(2,1)}, u32[]{:S(2)}, u32[]{:S(2)}) collective-permute-start(bf16[208,128]{1,0:T(8,128)(2,1)} %get-tuple-element.28), channel_id=1, source_target_pairs={{0,160},{32,192},{64,224},{96,0},{128,32},{160,64},{192,96},{224,1... | collective-permute-start | bytes 159752 | tf_op jit(solution)/shard_map/ppermute | solution.py:175
  52.0 3.2 %collective-permute-done.4.refs_5_ = bf16[208,128]{1,0:T(8,128)(2,1)} collective-permute-done((bf16[208,128]{1,0:T(8,128)(2,1)}, bf16[208,128]{1,0:T(8,128)(2,1)}, u32[]{:S(2)}, u32[]{:S(2)}) %collective-permute-start.4) | collective-permute-done | bytes 53280 | tf_op jit(solution)/shard_map/ppermute | solution.py:175
  55.2 4.8 %collective-permute-start.5 = (bf16[208,128]{1,0:T(8,128)(2,1)}, bf16[208,128]{1,0:T(8,128)(2,1)}, u32[]{:S(2)}, u32[]{:S(2)}) collective-permute-start(bf16[208,128]{1,0:T(8,128)(2,1)} %get-tuple-element.29), channel_id=1, source_target_pairs={{0,192},{32,224},{64,0},{96,32},{128,64},{160,96},{192,128},{224,1... | collective-permute-start | bytes 159752 | tf_op jit(solution)/shard_map/ppermute | solution.py:175
  64.0 2.6 %collective-permute-done.6.refs_7_ = bf16[208,128]{1,0:T(8,128)(2,1)} collective-permute-done((bf16[208,128]{1,0:T(8,128)(2,1)}, bf16[208,128]{1,0:T(8,128)(2,1)}, u32[]{:S(2)}, u32[]{:S(2)}) %collective-permute-start.6) | collective-permute-done | bytes 53280 | tf_op jit(solution)/shard_map/ppermute | solution.py:175
  73.0 3.7 %shard_map.127 = (f32[512,256]{1,0:T(8,128)S(1)}, bf16[512,256]{1,0:T(8,128)(2,1)}, bf16[512,256]{1,0:T(8,128)(2,1)}, bf16[512,256]{1,0:T(8,128)(2,1)}) custom-call(bf16[256,1024]{1,0:T(8,128)(2,1)S(1)} %bitcast.36, bf16[256,1024]{1,0:T(8,128)(2,1)} %collective-permute-done.14.other_ref, bf16[4096,128]{1,0:T(8,128)(2,1)S(1)} %bitcast.30, ...), custom_call_target="tpu_custom_call" | custom-call | tf_op jit(solution)/shard_map/pallas_call | solution.py:347
  80.9 16.5 %shard_map.124 = bf16[8,64,128]{2,1,0:T(8,128)(2,1)} custom-call(bf16[208,128]{1,0:T(8,128)(2,1)S(1)} %copy-done.6, bf16[208,128]{1,0:T(8,128)(2,1)S(1)} %copy-done.8, bf16[208,128]{1,0:T(8,128)(2,1)} %collective-permute-done.1.refs_2_, bf16[208,128]{1,0:T(8,128)(2,1)} %collective-permute-done.2.refs_3_, bf16[208,128]{1,0:T(8,128)(2,1)} %collective-permute-done.3.refs_4_, ...), custom_call_target="tpu_custom_call" | custom-call | flops 4000000000 | bytes 2000000 | tf_op jit(solution)/shard_map/pallas_call | solution.py:113
  97.4 6.2 %all-to-all-start = ((bf16[8,64,128]{2,1,0:T(8,128)(2,1)}), bf16[8,64,128]{2,1,0:T(8,128)(2,1)S(1)}, u32[]{:S(2)}, u32[]{:S(2)}) async-start(bf16[8,64,128]{2,1,0:T(8,128)(2,1)} %shard_map.124), calls=%async_computation | async-start | bytes 262144 | tf_op jit(solution)/shard_map/all_to_all | solution.py:186
  108.5 2.4 %collective-permute-start.22 = (bf16[512,128]{1,0:T(8,128)(2,1)}, bf16[512,128]{1,0:T(8,128)(2,1)S(1)}, u32[]{:S(2)}, u32[]{:S(2)}) collective-permute-start(bf16[512,128]{1,0:T(8,128)(2,1)} %shard_map.128.h0_ref), channel_id=1, source_target_pairs={{0,4},{2,6},{4,0},{6,2},{1,5},{3,7},{5,1},{7,3},{8,12},{10,14},{12... | collective-permute-start | bytes 393224 | tf_op jit(solution)/shard_map/ppermute | solution.py:175
  112.7 2.9 %convolution_convert_fusion = bf16[128,4096]{1,0:T(8,128)(2,1)S(1)} fusion(bf16[512,128]{1,0:T(8,128)(2,1)S(1)} %bitcast.42, bf16[512,4096]{1,0:T(8,128)(2,1)} %param.15), kind=kOutput, calls=%fused_computation | convolution fusion | flops 537395200 | bytes 5373952 | tf_op jit(solution)/shard_map/dot_general | solution.py:188
  122.0 2.3 %shard_map.130 = bf16[256,1024]{1,0:T(8,128)(2,1)} custom-call(f32[256,1024]{1,0:T(8,128)} %copy-done.3, bf16[256,1024]{1,0:T(8,128)(2,1)} %copy-done.11), custom_call_target="tpu_custom_call" | custom-call | tf_op jit(solution)/shard_map/pallas_call | solution.py:410
  124.2 9.3 %all-to-all-start.2 = ((bf16[32,8,1024]{2,1,0:T(8,128)(2,1)}), bf16[32,8,1024]{2,1,0:T(8,128)(2,1)S(1)}, u32[]{:S(2)}, u32[]{:S(2)}) async-start(bf16[32,8,1024]{2,1,0:T(8,128)(2,1)} %bitcast.41), calls=%async_computation.2 | async-start | bytes 1048576 | tf_op jit(solution)/shard_map/all_to_all | solution.py:434
  135.9 2.7 %collective-permute-start.12 = (bf16[16,4096]{1,0:T(8,128)(2,1)S(1)}, bf16[16,4096]{1,0:T(8,128)(2,1)S(1)}, u32[]{:S(2)}, u32[]{:S(2)}) collective-permute-start(bf16[16,4096]{1,0:T(8,128)(2,1)S(1)} %get-tuple-element.46), channel_id=1, source_target_pairs={{0,4},{2,6},{4,0},{6,2},{1,5},{3,7},{5,1},{7,3},{8,12},{10,14},{12... | collective-permute-start | bytes 393224 | tf_op jit(solution)/shard_map/ppermute | solution.py:175
  139.8 10.8 %all-to-all-done.2 = bf16[32,8,1024]{2,1,0:T(8,128)(2,1)S(1)} async-done(((bf16[32,8,1024]{2,1,0:T(8,128)(2,1)}), bf16[32,8,1024]{2,1,0:T(8,128)(2,1)S(1)}, u32[]{:S(2)}, u32[]{:S(2)}) %all-to-all-start.2) | async-done | bytes 524320 | tf_op jit(solution)/shard_map/all_to_all | solution.py:434
  151.5 2.3 %shard_map.131 = (bf16[2,16,1024]{2,1,0:T(8,128)(2,1)}, bf16[2,16,1024]{2,1,0:T(8,128)(2,1)}, bf16[2,16,1024]{2,1,0:T(8,128)(2,1)}, bf16[2,16,1024]{2,1,0:T(8,128)(2,1)}) custom-call(s32[2,128]{1,0:T(2,128)} %bitcast.44, bf16[256,1024]{1,0:T(8,128)(2,1)} %bitcast.39), custom_call_target="tpu_custom_call" | custom-call | tf_op jit(solution)/shard_map/pallas_call | solution.py:259
  154.8 2.7 %collective-permute-start.26 = (bf16[2,16,1024]{2,1,0:T(8,128)(2,1)}, bf16[2,16,1024]{2,1,0:T(8,128)(2,1)S(1)}, u32[]{:S(2)}, u32[]{:S(2)}) collective-permute-start(bf16[2,16,1024]{2,1,0:T(8,128)(2,1)} %get-tuple-element.42), channel_id=1, source_target_pairs={{0,4},{2,6},{4,0},{6,2},{1,5},{3,7},{5,1},{7,3},{8,12},{10,14},{12... | collective-permute-start | bytes 196616 | tf_op jit(solution)/shard_map/ppermute | solution.py:175
  (93 shorter events, 48.5 us)
Async XLA Ops:
  3.5 31.5 %all-to-all-start.1 = ((bf16[32,8,1024]{2,1,0:T(8,128)(2,1)}), bf16[32,8,1024]{2,1,0:T(8,128)(2,1)S(1)}, u32[]{:S(2)}, u32[]{:S(2)}) async-start(bf16[32,8,1024]{2,1,0:T(8,128)(2,1)} %bitcast.40), calls=%async_computation.1 | async-start | bytes 1048576 | tf_op jit(solution)/shard_map/all_to_all | solution.py:425
  18.4 51.3 %collective-permute-start.15 = (bf16[3072,128]{1,0:T(8,128)(2,1)}, bf16[3072,128]{1,0:T(8,128)(2,1)S(1)}, u32[]{:S(2)}, u32[]{:S(2)}) collective-permute-start(bf16[3072,128]{1,0:T(8,128)(2,1)} %get-tuple-element.31), channel_id=1, source_target_pairs={{0,2},{2,4},{4,6},{6,0},{1,3},{3,5},{5,7},{7,1},{8,10},{10,12},{12... | collective-permute-start | bytes 2359304 | tf_op jit(solution)/shard_map/ppermute | solution.py:175
  20.1 50.7 %collective-permute-start.16 = (bf16[3072,128]{1,0:T(8,128)(2,1)}, bf16[3072,128]{1,0:T(8,128)(2,1)}, u32[]{:S(2)}, u32[]{:S(2)}) collective-permute-start(bf16[3072,128]{1,0:T(8,128)(2,1)} %get-tuple-element.32), channel_id=1, source_target_pairs={{0,4},{2,6},{4,0},{6,2},{1,5},{3,7},{5,1},{7,3},{8,12},{10,14},{12... | collective-permute-start | bytes 2359304 | tf_op jit(solution)/shard_map/ppermute | solution.py:175
  23.0 50.0 %collective-permute-start.17 = (bf16[3072,128]{1,0:T(8,128)(2,1)}, bf16[3072,128]{1,0:T(8,128)(2,1)}, u32[]{:S(2)}, u32[]{:S(2)}) collective-permute-start(bf16[3072,128]{1,0:T(8,128)(2,1)} %get-tuple-element.33), channel_id=1, source_target_pairs={{0,6},{2,0},{4,2},{6,4},{1,7},{3,1},{5,3},{7,5},{8,14},{10,8},{12,... | collective-permute-start | bytes 2359304 | tf_op jit(solution)/shard_map/ppermute | solution.py:175
  26.3 6.5 %collective-permute-start = (bf16[208,128]{1,0:T(8,128)(2,1)}, bf16[208,128]{1,0:T(8,128)(2,1)S(1)}, u32[]{:S(2)}, u32[]{:S(2)}) collective-permute-start(bf16[208,128]{1,0:T(8,128)(2,1)} %get-tuple-element.24), channel_id=1, source_target_pairs={{0,32},{32,64},{64,96},{96,128},{128,160},{160,192},{192,224},{224... | collective-permute-start | bytes 159752 | tf_op jit(solution)/shard_map/ppermute | solution.py:175
  27.8 7.2 %collective-permute-start.1 = (bf16[208,128]{1,0:T(8,128)(2,1)}, bf16[208,128]{1,0:T(8,128)(2,1)}, u32[]{:S(2)}, u32[]{:S(2)}) collective-permute-start(bf16[208,128]{1,0:T(8,128)(2,1)} %get-tuple-element.25), channel_id=1, source_target_pairs={{0,64},{32,96},{64,128},{96,160},{128,192},{160,224},{192,0},{224,... | collective-permute-start | bytes 159752 | tf_op jit(solution)/shard_map/ppermute | solution.py:175
  32.8 7.6 %collective-permute-start.2 = (bf16[208,128]{1,0:T(8,128)(2,1)}, bf16[208,128]{1,0:T(8,128)(2,1)}, u32[]{:S(2)}, u32[]{:S(2)}) collective-permute-start(bf16[208,128]{1,0:T(8,128)(2,1)} %get-tuple-element.26), channel_id=1, source_target_pairs={{0,96},{32,128},{64,160},{96,192},{128,224},{160,0},{192,32},{224,... | collective-permute-start | bytes 159752 | tf_op jit(solution)/shard_map/ppermute | solution.py:175
  35.0 38.0 %collective-permute-start.14 = (bf16[256,1024]{1,0:T(8,128)(2,1)S(1)}, bf16[256,1024]{1,0:T(8,128)(2,1)}, u32[]{:S(2)}, u32[]{:S(2)}) collective-permute-start(bf16[256,1024]{1,0:T(8,128)(2,1)S(1)} %bitcast.35), channel_id=1, source_target_pairs={{0,1},{1,0},{2,3},{3,2},{4,5},{5,4},{6,7},{7,6},{8,9},{9,8},{10,11... | collective-permute-start | bytes 1572872 | tf_op jit(solution)/shard_map/ppermute | solution.py:175
  40.4 8.4 %collective-permute-start.3 = (bf16[208,128]{1,0:T(8,128)(2,1)}, bf16[208,128]{1,0:T(8,128)(2,1)}, u32[]{:S(2)}, u32[]{:S(2)}) collective-permute-start(bf16[208,128]{1,0:T(8,128)(2,1)} %get-tuple-element.27), channel_id=1, source_target_pairs={{0,128},{32,160},{64,192},{96,224},{128,0},{160,32},{192,64},{224,... | collective-permute-start | bytes 159752 | tf_op jit(solution)/shard_map/ppermute | solution.py:175
  55.2 6.9 %collective-permute-start.5 = (bf16[208,128]{1,0:T(8,128)(2,1)}, bf16[208,128]{1,0:T(8,128)(2,1)}, u32[]{:S(2)}, u32[]{:S(2)}) collective-permute-start(bf16[208,128]{1,0:T(8,128)(2,1)} %get-tuple-element.29), channel_id=1, source_target_pairs={{0,192},{32,224},{64,0},{96,32},{128,64},{160,96},{192,128},{224,1... | collective-permute-start | bytes 159752 | tf_op jit(solution)/shard_map/ppermute | solution.py:175
  68.3 12.1 %collective-permute-start.7 = (bf16[8,144,128]{2,1,0:T(8,128)(2,1)}, bf16[8,144,128]{2,1,0:T(8,128)(2,1)S(1)}, u32[]{:S(2)}, u32[]{:S(2)}) collective-permute-start(bf16[8,144,128]{2,1,0:T(8,128)(2,1)} %shard_map.123), channel_id=1, source_target_pairs={{0,8},{8,16},{16,24},{24,0},{1,9},{9,17},{17,25},{25,1},{2,10},{10... | collective-permute-start | bytes 884744 | tf_op jit(solution)/shard_map/ppermute | solution.py:175
  69.7 11.1 %collective-permute-start.8 = (bf16[8,144,128]{2,1,0:T(8,128)(2,1)}, bf16[8,144,128]{2,1,0:T(8,128)(2,1)S(1)}, u32[]{:S(2)}, u32[]{:S(2)}) collective-permute-start(bf16[8,144,128]{2,1,0:T(8,128)(2,1)} %shard_map.123), channel_id=1, source_target_pairs={{0,16},{8,24},{16,0},{24,8},{1,17},{9,25},{17,1},{25,9},{2,18},{10... | collective-permute-start | bytes 884744 | tf_op jit(solution)/shard_map/ppermute | solution.py:175
  70.8 10.1 %collective-permute-start.9 = (bf16[8,144,128]{2,1,0:T(8,128)(2,1)}, bf16[8,144,128]{2,1,0:T(8,128)(2,1)S(1)}, u32[]{:S(2)}, u32[]{:S(2)}) collective-permute-start(bf16[8,144,128]{2,1,0:T(8,128)(2,1)} %shard_map.123), channel_id=1, source_target_pairs={{0,24},{8,0},{16,8},{24,16},{1,25},{9,1},{17,9},{25,17},{2,26},{10... | collective-permute-start | bytes 884744 | tf_op jit(solution)/shard_map/ppermute | solution.py:175
  77.5 26.1 %collective-permute-start.18 = (bf16[512,256]{1,0:T(8,128)(2,1)}, bf16[512,256]{1,0:T(8,128)(2,1)S(1)}, u32[]{:S(2)}, u32[]{:S(2)}) collective-permute-start(bf16[512,256]{1,0:T(8,128)(2,1)} %get-tuple-element.35), channel_id=1, source_target_pairs={{0,6},{2,0},{4,2},{6,4},{1,7},{3,1},{5,3},{7,5},{8,14},{10,8},{12,... | collective-permute-start | bytes 786440 | tf_op jit(solution)/shard_map/ppermute | solution.py:175
  79.3 24.4 %collective-permute-start.19 = (bf16[512,256]{1,0:T(8,128)(2,1)}, bf16[512,256]{1,0:T(8,128)(2,1)S(1)}, u32[]{:S(2)}, u32[]{:S(2)}) collective-permute-start(bf16[512,256]{1,0:T(8,128)(2,1)} %get-tuple-element.36), channel_id=1, source_target_pairs={{0,4},{2,6},{4,0},{6,2},{1,5},{3,7},{5,1},{7,3},{8,12},{10,14},{12... | collective-permute-start | bytes 786440 | tf_op jit(solution)/shard_map/ppermute | solution.py:175
  80.4 23.3 %collective-permute-start.20 = (bf16[512,256]{1,0:T(8,128)(2,1)}, bf16[512,256]{1,0:T(8,128)(2,1)S(1)}, u32[]{:S(2)}, u32[]{:S(2)}) collective-permute-start(bf16[512,256]{1,0:T(8,128)(2,1)} %get-tuple-element.37), channel_id=1, source_target_pairs={{0,2},{2,4},{4,6},{6,0},{1,3},{3,5},{5,7},{7,1},{8,10},{10,12},{12... | collective-permute-start | bytes 786440 | tf_op jit(solution)/shard_map/ppermute | solution.py:175
  97.4 15.3 %all-to-all-start = ((bf16[8,64,128]{2,1,0:T(8,128)(2,1)}), bf16[8,64,128]{2,1,0:T(8,128)(2,1)S(1)}, u32[]{:S(2)}, u32[]{:S(2)}) async-start(bf16[8,64,128]{2,1,0:T(8,128)(2,1)} %shard_map.124), calls=%async_computation | async-start | bytes 262144 | tf_op jit(solution)/shard_map/all_to_all | solution.py:186
  106.6 9.0 %collective-permute-start.21 = (bf16[512,128]{1,0:T(8,128)(2,1)}, bf16[512,128]{1,0:T(8,128)(2,1)S(1)}, u32[]{:S(2)}, u32[]{:S(2)}) collective-permute-start(bf16[512,128]{1,0:T(8,128)(2,1)} %shard_map.128.h0_ref), channel_id=1, source_target_pairs={{0,2},{2,4},{4,6},{6,0},{1,3},{3,5},{5,7},{7,1},{8,10},{10,12},{12... | collective-permute-start | bytes 393224 | tf_op jit(solution)/shard_map/ppermute | solution.py:175
  108.5 7.2 %collective-permute-start.22 = (bf16[512,128]{1,0:T(8,128)(2,1)}, bf16[512,128]{1,0:T(8,128)(2,1)S(1)}, u32[]{:S(2)}, u32[]{:S(2)}) collective-permute-start(bf16[512,128]{1,0:T(8,128)(2,1)} %shard_map.128.h0_ref), channel_id=1, source_target_pairs={{0,4},{2,6},{4,0},{6,2},{1,5},{3,7},{5,1},{7,3},{8,12},{10,14},{12... | collective-permute-start | bytes 393224 | tf_op jit(solution)/shard_map/ppermute | solution.py:175
  119.3 14.2 %collective-permute-start.10 = (bf16[4,16,4096]{2,1,0:T(8,128)(2,1)S(1)}, bf16[4,16,4096]{2,1,0:T(8,128)(2,1)S(1)}, u32[]{:S(2)}, u32[]{:S(2)}) collective-permute-start(bf16[4,16,4096]{2,1,0:T(8,128)(2,1)S(1)} %dynamic-slice_bitcast_fusion), channel_id=1, source_target_pairs={{0,1},{1,0},{2,3},{3,2},{4,5},{5,4},{6,7},{7,6},{8,9},{9,8},{10,11... | collective-permute-start | bytes 1572872 | tf_op jit(solution)/shard_map/ppermute | solution.py:175
  124.2 26.4 %all-to-all-start.2 = ((bf16[32,8,1024]{2,1,0:T(8,128)(2,1)}), bf16[32,8,1024]{2,1,0:T(8,128)(2,1)S(1)}, u32[]{:S(2)}, u32[]{:S(2)}) async-start(bf16[32,8,1024]{2,1,0:T(8,128)(2,1)} %bitcast.41), calls=%async_computation.2 | async-start | bytes 1048576 | tf_op jit(solution)/shard_map/all_to_all | solution.py:434
  134.7 22.8 %collective-permute-start.11 = (bf16[16,4096]{1,0:T(8,128)(2,1)S(1)}, bf16[16,4096]{1,0:T(8,128)(2,1)S(1)}, u32[]{:S(2)}, u32[]{:S(2)}) collective-permute-start(bf16[16,4096]{1,0:T(8,128)(2,1)S(1)} %get-tuple-element.44), channel_id=1, source_target_pairs={{0,2},{2,4},{4,6},{6,0},{1,3},{3,5},{5,7},{7,1},{8,10},{10,12},{12... | collective-permute-start | bytes 393224 | tf_op jit(solution)/shard_map/ppermute | solution.py:175
  135.9 22.2 %collective-permute-start.12 = (bf16[16,4096]{1,0:T(8,128)(2,1)S(1)}, bf16[16,4096]{1,0:T(8,128)(2,1)S(1)}, u32[]{:S(2)}, u32[]{:S(2)}) collective-permute-start(bf16[16,4096]{1,0:T(8,128)(2,1)S(1)} %get-tuple-element.46), channel_id=1, source_target_pairs={{0,4},{2,6},{4,0},{6,2},{1,5},{3,7},{5,1},{7,3},{8,12},{10,14},{12... | collective-permute-start | bytes 393224 | tf_op jit(solution)/shard_map/ppermute | solution.py:175
  138.6 19.5 %collective-permute-start.13 = (bf16[16,4096]{1,0:T(8,128)(2,1)S(1)}, bf16[16,4096]{1,0:T(8,128)(2,1)S(1)}, u32[]{:S(2)}, u32[]{:S(2)}) collective-permute-start(bf16[16,4096]{1,0:T(8,128)(2,1)S(1)} %get-tuple-element.45), channel_id=1, source_target_pairs={{0,6},{2,0},{4,2},{6,4},{1,7},{3,1},{5,3},{7,5},{8,14},{10,8},{12,... | collective-permute-start | bytes 393224 | tf_op jit(solution)/shard_map/ppermute | solution.py:175
  (26 other events, 341.6 us)
where the time goes:
time: 165 us; the launch traced here: 164 us
  starting transfers between devices  76.2 us (46%)
  Pallas kernels  40.5 us (25%)
  waiting for transfers between devices  36.2 us (22%)
  local copies, waits for them, and re-layouts  5.62 us (3%)
  matrix products  2.93 us (2%)
  other arithmetic  1.9 us (1%)
    ppermute x28, starting transfers between devices, shifted(): lax.ppermute(value, axis, [(i, (i + by) % size) for i in range(size)])  49.1 us
    ppermute x28, waiting for transfers between devices, shifted(): lax.ppermute(value, axis, [(i, (i + by) % size) for i in range(size)])  24.6 us
    pallas_call x1, Pallas kernels, attend(): pl.pallas_call(attend_kernel, out_shape=jax.ShapeDtypeStruct((8, HEAD, 12...  16.5 us
    all_to_all x1, starting transfers between devices, experts(): lax.all_to_all(outgoing, ep, split_axis=0, concat_axis=0, tiled=True)  11.6 us
    all_to_all x1, waiting for transfers between devices, experts(): lax.all_to_all(result.reshape(Z * X, 8, width), ep, split_axis=0, concat_...  10.8 us
    all_to_all x1, starting transfers between devices, experts(): lax.all_to_all(result.reshape(Z * X, 8, width), ep, split_axis=0, concat_...  9.27 us
    all_to_all x1, starting transfers between devices, mixer(): attended = lax.all_to_all(out, 'z', split_axis=0, concat_axis=0, tiled=True)  6.25 us
    unnamed x39, local copies, waits for them, and re-layouts  5.55 us
  transfers between devices with their start and end apart: 31, of which 14 were waited for; matrix products, arithmetic and copies ran while one was open for 3% of the time, Pallas kernels for 21%

commit v1 on v0

--- a/solution.py
+++ b/solution.py
@@ -37,9 +37,7 @@
             kv_ref[lax.rem(here + (X - shift), X), at] = piece[i]
     row = lax.broadcasted_iota(jnp.int32, (256, 256), 0)
     col = lax.broadcasted_iota(jnp.int32, (256, 256), 1)
-    tri = jnp.where(row > col, 1.0, 0.0).astype(BF)
-    tri_ref[0:256] = tri
-    tri_ref[256:512] = tri
+    tri_ref[...] = jnp.where(row > col, 1.0, 0.0).astype(BF)
     ones = jnp.where(lax.broadcasted_iota(jnp.int32, (64, 128), 0) == 0, 1.0, 0.0)
     for i in range(Z):
         q = jnp.concatenate([arrived[i][:HEAD].astype(F32), ones], axis=0)
@@ -58,20 +56,17 @@
         sp = jnp.maximum(s, jnp.log(1.0 + jnp.exp(jnp.minimum(s, 80.0))))
         if mask is not None:
             sp = jnp.where(mask, sp, 0.0)
-        high = sp.astype(BF)
-        low = (sp - high.astype(F32)).astype(BF)
+        rounded = sp.astype(BF)
         logit = s - sp
         weights = [None, None]
         for half in (1, 0):
             at = slice(half * 256, half * 256 + 256)
-            after = jnp.dot(
-                jnp.concatenate([high[:, at], low[:, at]], axis=1), tri_ref[...], preferred_element_type=F32
-            )
-            w = jnp.exp(logit[:, at] - after - carry)
+            behind = jnp.dot(rounded[:, at], tri_ref[...], preferred_element_type=F32)
+            w = jnp.exp(logit[:, at] - behind - carry)
             if mask is not None:
                 w = jnp.where(mask[:, at], w, 0.0)
             weights[half] = w.astype(BF)
-            carry = carry + after[:, 0:1] + sp[:, half * 256 : half * 256 + 1]
+            carry = carry + behind[:, 0:1] + sp[:, half * 256 : half * 256 + 1]
         values = jnp.concatenate([kv_ref[i, t, 80:144, :] for i in range(4)], axis=1)
         out = lax.dot_general(
             jnp.concatenate(weights, axis=1), values, (((1,), (1,)), ((), ())), preferred_element_type=F32
@@ -118,7 +113,7 @@
         scratch_shapes=[
             pltpu.VMEM((4, 8, 144, 128), BF),
             pltpu.VMEM((8, 128, 128), BF),
-            pltpu.VMEM((512, 256), BF),
+            pltpu.VMEM((256, 256), BF),
             pltpu.VMEM((8, 128, 1), F32),
             pltpu.VMEM((8, 128, HEAD), F32),
             pltpu.SMEM((len(STEPS), 8), jnp.int32),
@@ -265,12 +260,27 @@
     )(ids, rows)
 
 
+def spread_kernel(weights_ref, out_ref):
+    w = weights_ref[...]
+    for k in range(2):
+        out_ref[k] = jnp.broadcast_to(w[:, k : k + 1], (16, 128))
+
+
+def spread_weights(weights):
+    return pl.pallas_call(
+        spread_kernel,
+        out_shape=jax.ShapeDtypeStruct((2, 16, 128), F32),
+        in_specs=[VMEM],
+        out_specs=VMEM,
+    )(weights)
+
+
 def finish_kernel(p0_ref, p1_ref, p2_ref, p3_ref, weights_ref, out_ref):
-    w = weights_ref[...]
     width = p0_ref.shape[2]
+    w = [jnp.concatenate([weights_ref[k]] * (width // 128), axis=1) for k in range(2)]
     for s, p in enumerate((p0_ref, p1_ref, p2_ref, p3_ref)):
         at = pl.multiple_of(lax.rem(lax.axis_index("y") + (Y - s), Y) * width, width)
-        total = p[0].astype(F32) * w[:, 0:1] + p[1].astype(F32) * w[:, 1:2]
+        total = p[0].astype(F32) * w[0] + p[1].astype(F32) * w[1]
         out_ref[:, pl.ds(at, width)] = total.astype(BF)
 
 
@@ -283,10 +293,10 @@
     )(*picked, weights)
 
 
-def share_kernel(gate_ref, up_ref, down_ref, o1_ref, o2_ref, o3_ref, sem):
+def share_kernel(gate_ref, up_ref, down_ref, o0_ref, o1_ref, o2_ref, o3_ref, sem):
     width = gate_ref.shape[0] // Y
     copies = []
-    for s, out in ((1, o1_ref), (2, o2_ref), (3, o3_ref)):
+    for s, out in ((1, o1_ref), (2, o2_ref), (3, o3_ref), (0, o0_ref)):
         start = pl.multiple_of(lax.rem(lax.axis_index("y") + s, Y) * width, width)
         copies.append((gate_ref.at[pl.ds(start, width), :], out.at[pl.ds(0, width), :]))
         copies.append((up_ref.at[pl.ds(start, width), :], out.at[pl.ds(width, width), :]))
@@ -309,110 +319,76 @@
     out = jax.ShapeDtypeStruct((3 * width, 128), BF)
     return pl.pallas_call(
         share_kernel,
-        out_shape=[out] * (Y - 1),
+        out_shape=[out] * Y,
         in_specs=[ANY, ANY, ANY],
-        out_specs=[VMEM] * (Y - 1),
-        scratch_shapes=[pltpu.SemaphoreType.DMA(((Y - 1) * (2 + width // 128),))],
+        out_specs=[VMEM] * Y,
+        scratch_shapes=[pltpu.SemaphoreType.DMA((Y * (2 + width // 128),))],
     )(gate, up, down)
 
 
-def expand_kernel(
-    own_ref, other_ref, gate_ref, up_ref, w1_ref, w2_ref, w3_ref, o0_ref, o1_ref, o2_ref, o3_ref, kept_ref, sem
-):
-    width = own_ref.shape[1]
-    rows = own_ref.shape[0]
-    start = pl.multiple_of(lax.axis_index("y") * width, width)
-    copies = [
-        pltpu.make_async_copy(ref.at[pl.ds(start, width), :], kept_ref.at[n], sem.at[n])
-        for n, ref in enumerate((gate_ref, up_ref))
-    ]
-    for copy in copies:
-        copy.start()
-
-    def into(o_ref, w):
-        o_ref[0:rows] = jnp.dot(own_ref[...], w, preferred_element_type=F32).astype(o_ref.dtype)
-        o_ref[rows : 2 * rows] = jnp.dot(other_ref[...], w, preferred_element_type=F32).astype(o_ref.dtype)
-
-    for w_ref, o_ref in ((w1_ref, o1_ref), (w2_ref, o2_ref), (w3_ref, o3_ref)):
-        into(o_ref, jnp.concatenate([w_ref[0:width], w_ref[width : 2 * width]], axis=1))
-    for copy in copies:
-        copy.wait()
-    into(o0_ref, jnp.concatenate([kept_ref[0], kept_ref[1]], axis=1))
-
-
-def expand(own, other, gate, up, shared):
-    rows = 2 * own.shape[0]
-    width = own.shape[1]
-    sent = jax.ShapeDtypeStruct((rows, 256), BF)
+def expand_kernel(*refs):
+    rows_ref, ours, theirs, outs = refs[0], refs[1 : 1 + Y], refs[1 + Y : 1 + 2 * Y], refs[1 + 2 * Y :]
+    width = rows_ref.shape[1]
+    for s in (1, 2, 3, 0):
+        parts = []
+        for w_ref in (ours[s], theirs[s]):
+            w = jnp.concatenate([w_ref[0:width], w_ref[width : 2 * width]], axis=1)
+            parts.append(jnp.dot(rows_ref[...], w, preferred_element_type=F32))
+        outs[s][...] = jnp.concatenate(parts, axis=1).astype(outs[s].dtype)
+
+
+def expand(rows, ours, theirs):
+    sent = jax.ShapeDtypeStruct((rows.shape[0], 512), BF)
     return pl.pallas_call(
         expand_kernel,
-        out_shape=[jax.ShapeDtypeStruct((rows, 256), F32), sent, sent, sent],
-        in_specs=[VMEM, VMEM, ANY, ANY] + [VMEM] * 3,
-        out_specs=[VMEM] * 4,
-        scratch_shapes=[pltpu.VMEM((2, width, 128), BF), pltpu.SemaphoreType.DMA((2,))],
+        out_shape=[jax.ShapeDtypeStruct((rows.shape[0], 512), F32), sent, sent, sent],
+        in_specs=[VMEM] * (1 + 2 * Y),
+        out_specs=[VMEM] * Y,
         compiler_params=pltpu.CompilerParams(vmem_limit_bytes=32 * 1024 * 1024),
-    )(own, other, gate, up, *shared)
+    )(rows, *ours, *theirs)
 
 
 def hidden_kernel(p0_ref, p1_ref, p2_ref, p3_ref, o_ref):
-    both = p0_ref[...]
-    for p in (p1_ref, p2_ref, p3_ref):
-        both = both + p[...].astype(F32)
-    gate, up = both[:, 0:128], both[:, 128:256]
-    o_ref[...] = (gate / (1.0 + jnp.exp(-gate)) * up).astype(BF)
+    for n in range(C):
+        both = p0_ref[:, n * 256 : n * 256 + 256]
+        for p in (p1_ref, p2_ref, p3_ref):
+            both = both + p[:, n * 256 : n * 256 + 256].astype(F32)
+        gate, up = both[:, 0:128], both[:, 128:256]
+        o_ref[:, n * 128 : n * 128 + 128] = (gate / (1.0 + jnp.exp(-gate)) * up).astype(BF)
 
 
 def hidden_units(parts):
     return pl.pallas_call(
         hidden_kernel,
-        out_shape=jax.ShapeDtypeStruct((parts[0].shape[0], 128), BF),
+        out_shape=jax.ShapeDtypeStruct((parts[0].shape[0], 256), BF),
         in_specs=[VMEM] * 4,
         out_specs=VMEM,
     )(*parts)
 
 
-def reduce_kernel(
-    h0_ref, h1_ref, h2_ref, h3_ref, down_ref, w1_ref, w2_ref, w3_ref, own_ref, other_ref, kept_ref, sem
-):
-    rows, width = own_ref.shape
-    start = pl.multiple_of(lax.axis_index("y") * width, width)
-    copy = pltpu.make_async_copy(down_ref.at[:, pl.ds(start, width)], kept_ref, sem)
-    copy.start()
-    units = jnp.concatenate([h[...] for h in (h1_ref, h2_ref, h3_ref, h0_ref)], axis=1)
+def reduce_kernel(*refs):
+    units, ours, theirs, o_ref = refs[:Y], refs[Y : 2 * Y], refs[2 * Y : 3 * Y], refs[3 * Y]
+    width = o_ref.shape[1]
     columns = []
-    for w_ref in (w1_ref, w2_ref, w3_ref):
-        blocks = [w_ref[2 * width + j * 128 : 2 * width + j * 128 + 128] for j in range(width // 128)]
-        columns.append(jnp.concatenate(blocks, axis=1))
-    copy.wait()
-    w = jnp.concatenate(columns + [kept_ref[...]], axis=0)
-    other_ref[...] = jnp.dot(units[rows:], w, preferred_element_type=F32).astype(BF)
-    own_ref[...] = jnp.dot(units[:rows], w, preferred_element_type=F32)
-
-
-def reduce_units(units, down, shared):
-    rows = units[0].shape[0] // 2
-    width = shared[0].shape[0] // 3
+    for s in range(Y):
+        for w_ref in (ours[s], theirs[s]):
+            blocks = [w_ref[2 * width + j * 128 : 2 * width + j * 128 + 128] for j in range(width // 128)]
+            columns.append(jnp.concatenate(blocks, axis=1))
+    w = jnp.concatenate(columns, axis=0)
+    h = jnp.concatenate([u[...] for u in units], axis=1)
+    o_ref[...] = jnp.dot(h, w, preferred_element_type=F32).astype(BF)
+
+
+def reduce_units(units, ours, theirs):
+    rows = units[0].shape[0]
+    width = ours[0].shape[0] // 3
     return pl.pallas_call(
         reduce_kernel,
-        out_shape=[jax.ShapeDtypeStruct((rows, width), F32), jax.ShapeDtypeStruct((rows, width), BF)],
-        in_specs=[VMEM] * 4 + [ANY] + [VMEM] * 3,
-        out_specs=[VMEM] * 2,
-        scratch_shapes=[pltpu.VMEM((128, width), BF), pltpu.SemaphoreType.DMA],
+        out_shape=jax.ShapeDtypeStruct((rows, width), BF),
+        in_specs=[VMEM] * (3 * Y),
+        out_specs=VMEM,
         compiler_params=pltpu.CompilerParams(vmem_limit_bytes=32 * 1024 * 1024),
-    )(*units, down, *shared)
-
-
-def add_kernel(a_ref, b_ref, o_ref):
-    o_ref[...] = (a_ref[...] + b_ref[...].astype(F32)).astype(BF)
-
-
-def added(a, b):
-    return pl.pallas_call(
-        add_kernel,
-        out_shape=jax.ShapeDtypeStruct(a.shape, BF),
-        in_specs=[VMEM, VMEM],
-        out_specs=VMEM,
-    )(a, b)
+    )(*units, *ours, *theirs)
 
 
 def experts(routed_rows, expert_ids, route_weights, gate_weight, up_weight, down_weight):
@@ -420,23 +396,22 @@
     ids = expert_ids.T
     width = routed_rows.shape[1] // Y
     kept = share(gate_weight[0], up_weight[0], down_weight[0])
-    shared = [shifted(kept[s - 1], "y", Y, s) for s in (1, 2, 3)]
+    ours = [kept[0]] + [shifted(kept[s], "y", Y, s) for s in (1, 2, 3)]
+    theirs = [shifted(w, "c", C, 1) for w in ours]
     outgoing = dispatch(ids, routed_rows).reshape(Z * X, 8, width)
     own = lax.all_to_all(outgoing, ep, split_axis=0, concat_axis=0, tiled=True).reshape(256, width)
-    other = shifted(own, "c", C, 1)
-    parts = expand(own, other, gate_weight[0], up_weight[0], shared)
+    wide = spread_weights(route_weights)
+    parts = expand(own, ours, theirs)
     summed = [parts[0]] + [shifted(parts[s], "y", Y, Y - s) for s in (1, 2, 3)]
     mine = hidden_units(summed)
     units = [mine] + [shifted(mine, "y", Y, s) for s in (1, 2, 3)]
-    own_out, other_out = reduce_units(units, down_weight[0], shared)
-    other_out = shifted(other_out, "c", C, 1)
-    result = added(own_out, other_out)
+    result = reduce_units(units, ours, theirs)
     returned = lax.all_to_all(
         result.reshape(Z * X, 8, width), ep, split_axis=0, concat_axis=0, tiled=True
     ).reshape(256, width)
     picked = collect(ids, returned)
     picked = [picked[0]] + [shifted(picked[s], "y", Y, s) for s in (1, 2, 3)]
-    return finish(picked, route_weights)
+    return finish(picked, wide)
 
 
 def shards(

time: 165 us -> 175 us (1.061)
  waiting for transfers between devices: 36.2 us -> 51.2 us
  starting transfers between devices: 76.2 us -> 64.1 us
  local copies, waits for them, and re-layouts: 5.62 us -> 14.3 us
  Pallas kernels: 40.5 us -> 38.6 us
    all_to_all x1, waiting for transfers between devices: 0.01 us -> 9.88 us  [experts(): lax.all_to_all(outgoing, ep, split_axis=0, concat_axis=0, tiled=True)]
    unnamed x39 -> x57, local copies, waits for them, and re-layouts: 5.55 us -> 13.4 us
    all_to_all x1, starting transfers between devices: 11.6 us -> 4.89 us  [experts(): lax.all_to_all(outgoing, ep, split_axis=0, concat_axis=0, tiled=True)]
    all_to_all x1, waiting for transfers between devices: 0.77 us -> 6.33 us  [mixer(): attended = lax.all_to_all(out, 'z', split_axis=0, concat_axis=0, tiled=True)]
    all_to_all x1, starting transfers between devices: 6.25 us -> 3.57 us  [mixer(): attended = lax.all_to_all(out, 'z', split_axis=0, concat_axis=0, tiled=True)]
    ppermute x28 -> x30, starting transfers between devices: 49.1 us -> 46.6 us  [shifted(): lax.ppermute(value, axis, [(i, (i + by) % size) for i in range(size)])]
    all_to_all x1, waiting for transfers between devices: 10.8 us -> 8.6 us  [experts(): lax.all_to_all(result.reshape(Z * X, 8, width), ep, split_axis=0, concat_...]
    ppermute x28 -> x30, waiting for transfers between devices: 24.6 us -> 26.4 us  [shifted(): lax.ppermute(value, axis, [(i, (i + by) % size) for i in range(size)])]
  transfers between devices with their start and end apart: 31 -> 33, of which waited for: 14 -> 14; matrix products, arithmetic and copies ran while one was open for 3% -> 4% of each run, Pallas kernels for 21% -> 19%
where the time goes in v1:
time: 175 us; the launch traced here: 174 us
  starting transfers between devices  64.1 us (37%)
  waiting for transfers between devices  51.2 us (29%)
  Pallas kernels  38.6 us (22%)
  local copies, waits for them, and re-layouts  14.3 us (8%)
  matrix products  2.93 us (2%)
  other arithmetic  2.06 us (1%)
    ppermute x30, starting transfers between devices, shifted(): lax.ppermute(value, axis, [(i, (i + by) % size) for i in range(size)])  46.6 us
    ppermute x30, waiting for transfers between devices, shifted(): lax.ppermute(value, axis, [(i, (i + by) % size) for i in range(size)])  26.4 us
    pallas_call x1, Pallas kernels, attend(): pl.pallas_call(attend_kernel, out_shape=jax.ShapeDtypeStruct((8, HEAD, 12...  15.1 us
    unnamed x57, local copies, waits for them, and re-layouts  13.4 us
    all_to_all x1, waiting for transfers between devices, experts(): lax.all_to_all(outgoing, ep, split_axis=0, concat_axis=0, tiled=True)  9.88 us
    all_to_all x1, starting transfers between devices, experts(): lax.all_to_all(result.reshape(Z * X, 8, width), ep, split_axis=0, concat_...  9.04 us
    all_to_all x1, waiting for transfers between devices, experts(): lax.all_to_all(result.reshape(Z * X, 8, width), ep, split_axis=0, concat_...  8.6 us
    all_to_all x1, waiting for transfers between devices, mixer(): attended = lax.all_to_all(out, 'z', split_axis=0, concat_axis=0, tiled=True)  6.33 us
  transfers between devices with their start and end apart: 33, of which 14 were waited for; matrix products, arithmetic and copies ran while one was open for 4% of the time, Pallas kernels for 19%

profile of v1, /device:TPU:2, one launch (start us, length us, event | category | flops | bytes accessed | tf_op | source)
XLA Modules:
  0.0 174.1 jit_solution(10369611480397062578)
XLA Ops:
  4.5 3.3 %collective-permute-start.1 = (bf16[208,128]{1,0:T(8,128)(2,1)}, bf16[208,128]{1,0:T(8,128)(2,1)S(1)}, u32[]{:S(2)}, u32[]{:S(2)}) collective-permute-start(bf16[208,128]{1,0:T(8,128)(2,1)} %get-tuple-element.24), channel_id=1, source_target_pairs={{0,64},{32,96},{64,128},{96,160},{128,192},{160,224},{192,0},{224,... | collective-permute-start | bytes 159752 | tf_op jit(solution)/shard_map/ppermute | solution.py:170
  7.8 4.0 %collective-permute-start.2 = (bf16[208,128]{1,0:T(8,128)(2,1)}, bf16[208,128]{1,0:T(8,128)(2,1)S(1)}, u32[]{:S(2)}, u32[]{:S(2)}) collective-permute-start(bf16[208,128]{1,0:T(8,128)(2,1)} %get-tuple-element.25), channel_id=1, source_target_pairs={{0,96},{32,128},{64,160},{96,192},{128,224},{160,0},{192,32},{224,... | collective-permute-start | bytes 159752 | tf_op jit(solution)/shard_map/ppermute | solution.py:170
  12.4 4.9 %collective-permute-start.4 = (bf16[208,128]{1,0:T(8,128)(2,1)}, bf16[208,128]{1,0:T(8,128)(2,1)S(1)}, u32[]{:S(2)}, u32[]{:S(2)}) collective-permute-start(bf16[208,128]{1,0:T(8,128)(2,1)} %get-tuple-element.27), channel_id=1, source_target_pairs={{0,160},{32,192},{64,224},{96,0},{128,32},{160,64},{192,96},{224,1... | collective-permute-start | bytes 159752 | tf_op jit(solution)/shard_map/ppermute | solution.py:170
  17.4 2.7 %collective-permute-start.5 = (bf16[208,128]{1,0:T(8,128)(2,1)}, bf16[208,128]{1,0:T(8,128)(2,1)S(1)}, u32[]{:S(2)}, u32[]{:S(2)}) collective-permute-start(bf16[208,128]{1,0:T(8,128)(2,1)} %get-tuple-element.28), channel_id=1, source_target_pairs={{0,192},{32,224},{64,0},{96,32},{128,64},{160,96},{192,128},{224,1... | collective-permute-start | bytes 159752 | tf_op jit(solution)/shard_map/ppermute | solution.py:170
  21.1 3.7 %collective-permute-done.4.refs_5_ = bf16[208,128]{1,0:T(8,128)(2,1)S(1)} collective-permute-done((bf16[208,128]{1,0:T(8,128)(2,1)}, bf16[208,128]{1,0:T(8,128)(2,1)S(1)}, u32[]{:S(2)}, u32[]{:S(2)}) %collective-permute-start.4) | collective-permute-done | bytes 53280 | tf_op jit(solution)/shard_map/ppermute | solution.py:170
  32.7 3.8 %shard_map.126 = (bf16[3072,128]{1,0:T(8,128)(2,1)}, bf16[3072,128]{1,0:T(8,128)(2,1)}, bf16[3072,128]{1,0:T(8,128)(2,1)}, bf16[3072,128]{1,0:T(8,128)(2,1)}) custom-call(bf16[4096,128]{1,0:T(8,128)(2,1)} %bitcast.34, bf16[4096,128]{1,0:T(8,128)(2,1)} %bitcast.35, bf16[128,4096]{1,0:T(8,128)(2,1)} %bitcast.36), custom_call_target="tpu_custom_call" | custom-call | tf_op jit(solution)/shard_map/pallas_call | solution.py:320
  38.2 2.9 %collective-permute-start.15 = (bf16[3072,128]{1,0:T(8,128)(2,1)}, bf16[3072,128]{1,0:T(8,128)(2,1)S(1)}, u32[]{:S(2)}, u32[]{:S(2)}) collective-permute-start(bf16[3072,128]{1,0:T(8,128)(2,1)} %get-tuple-element.32), channel_id=1, source_target_pairs={{0,4},{2,6},{4,0},{6,2},{1,5},{3,7},{5,1},{7,3},{8,12},{10,14},{12... | collective-permute-start | bytes 2359304 | tf_op jit(solution)/shard_map/ppermute | solution.py:170
  51.3 15.1 %shard_map.124 = bf16[8,64,128]{2,1,0:T(8,128)(2,1)} custom-call(bf16[208,128]{1,0:T(8,128)(2,1)S(1)} %copy-done.4, bf16[208,128]{1,0:T(8,128)(2,1)S(1)} %copy-done.6, bf16[208,128]{1,0:T(8,128)(2,1)S(1)} %copy-done.8, bf16[208,128]{1,0:T(8,128)(2,1)S(1)} %copy-done.10, bf16[208,128]{1,0:T(8,128)(2,1)S(1)} %copy-done.12, bf16[208,128]{1,0:T(8,128)(2,1)S(1)} %copy-done.14, ...), custom_call_target="tpu_custom_call" | custom-call | flops 4000000000 | bytes 2000000 | tf_op jit(solution)/shard_map/pallas_call | solution.py:108
  66.4 3.6 %all-to-all-start = ((bf16[8,64,128]{2,1,0:T(8,128)(2,1)}), bf16[8,64,128]{2,1,0:T(8,128)(2,1)S(1)}, u32[]{:S(2)}, u32[]{:S(2)}) async-start(bf16[8,64,128]{2,1,0:T(8,128)(2,1)} %shard_map.124), calls=%async_computation | async-start | bytes 262144 | tf_op jit(solution)/shard_map/all_to_all | solution.py:181
  69.9 2.7 %shard_map.125 = bf16[256,1024]{1,0:T(8,128)(2,1)} custom-call(s32[2,128]{1,0:T(2,128)} %bitcast.38, bf16[128,4096]{1,0:T(8,128)(2,1)} %rows_ref.1), custom_call_target="tpu_custom_call" | custom-call | tf_op jit(solution)/shard_map/pallas_call | solution.py:233
  72.7 6.3 %all-to-all-done = bf16[8,64,128]{2,1,0:T(8,128)(2,1)S(1)} async-done(((bf16[8,64,128]{2,1,0:T(8,128)(2,1)}), bf16[8,64,128]{2,1,0:T(8,128)(2,1)S(1)}, u32[]{:S(2)}, u32[]{:S(2)}) %all-to-all-start) | async-done | bytes 131104 | tf_op jit(solution)/shard_map/all_to_all | solution.py:181
  79.0 4.9 %all-to-all-start.1 = ((bf16[32,8,1024]{2,1,0:T(8,128)(2,1)}), bf16[32,8,1024]{2,1,0:T(8,128)(2,1)}, u32[]{:S(2)}, u32[]{:S(2)}) async-start(bf16[32,8,1024]{2,1,0:T(8,128)(2,1)} %bitcast.33), calls=%async_computation.1 | async-start | bytes 1048576 | tf_op jit(solution)/shard_map/all_to_all | solution.py:402
  85.0 2.9 %convolution_convert_fusion = bf16[128,4096]{1,0:T(8,128)(2,1)S(1)} fusion(bf16[512,128]{1,0:T(8,128)(2,1)S(1)} %bitcast.37, bf16[512,4096]{1,0:T(8,128)(2,1)} %param.15), kind=kOutput, calls=%fused_computation | convolution fusion | flops 537395200 | bytes 5373952 | tf_op jit(solution)/shard_map/dot_general | solution.py:183
  89.9 9.9 %all-to-all-done.1 = bf16[32,8,1024]{2,1,0:T(8,128)(2,1)} async-done(((bf16[32,8,1024]{2,1,0:T(8,128)(2,1)}), bf16[32,8,1024]{2,1,0:T(8,128)(2,1)}, u32[]{:S(2)}, u32[]{:S(2)}) %all-to-all-start.1) | async-done | bytes 524320 | tf_op jit(solution)/shard_map/all_to_all | solution.py:402
  99.8 3.3 %shard_map.127 = (f32[256,512]{1,0:T(8,128)S(1)}, bf16[256,512]{1,0:T(8,128)(2,1)S(1)}, bf16[256,512]{1,0:T(8,128)(2,1)S(1)}, bf16[256,512]{1,0:T(8,128)(2,1)S(1)}) custom-call(bf16[256,1024]{1,0:T(8,128)(2,1)} %bitcast.11.refs_0_, bf16[3072,128]{1,0:T(8,128)(2,1)S(1)} %copy-done, bf16[3072,128]{1,0:T(8,128)(2,1)S(1)} %collective-permute-done.14.refs_2_.refs_5_, ...), custom_call_target="tpu_custom_call" | custom-call | tf_op jit(solution)/shard_map/pallas_call | solution.py:342
  103.9 3.0 %collective-permute-start.21 = (bf16[256,512]{1,0:T(8,128)(2,1)S(1)}, bf16[256,512]{1,0:T(8,128)(2,1)S(1)}, u32[]{:S(2)}, u32[]{:S(2)}) collective-permute-start(bf16[256,512]{1,0:T(8,128)(2,1)S(1)} %get-tuple-element.35), channel_id=1, source_target_pairs={{0,6},{2,0},{4,2},{6,4},{1,7},{3,1},{5,3},{7,5},{8,14},{10,8},{12,... | collective-permute-start | bytes 786440 | tf_op jit(solution)/shard_map/ppermute | solution.py:170
  108.5 6.6 %collective-permute-done.21.p1_ref = bf16[256,512]{1,0:T(8,128)(2,1)S(1)} collective-permute-done((bf16[256,512]{1,0:T(8,128)(2,1)S(1)}, bf16[256,512]{1,0:T(8,128)(2,1)S(1)}, u32[]{:S(2)}, u32[]{:S(2)}) %collective-permute-start.21) | collective-permute-done | bytes 262176 | tf_op jit(solution)/shard_map/ppermute | solution.py:170
  116.2 2.7 %collective-permute-done.23.p3_ref = bf16[256,512]{1,0:T(8,128)(2,1)S(1)} collective-permute-done((bf16[256,512]{1,0:T(8,128)(2,1)S(1)}, bf16[256,512]{1,0:T(8,128)(2,1)S(1)}, u32[]{:S(2)}, u32[]{:S(2)}) %collective-permute-start.23) | collective-permute-done | bytes 262176 | tf_op jit(solution)/shard_map/ppermute | solution.py:170
  125.0 4.8 %collective-permute-done.24.refs_1_ = bf16[256,256]{1,0:T(8,128)(2,1)S(1)} collective-permute-done((bf16[256,256]{1,0:T(8,128)(2,1)}, bf16[256,256]{1,0:T(8,128)(2,1)S(1)}, u32[]{:S(2)}, u32[]{:S(2)}) %collective-permute-start.24) | collective-permute-done | bytes 131104 | tf_op jit(solution)/shard_map/ppermute | solution.py:170
  131.3 2.5 %shard_map.129 = bf16[256,1024]{1,0:T(8,128)(2,1)S(1)} custom-call(bf16[256,256]{1,0:T(8,128)(2,1)S(1)} %copy-done.2, bf16[256,256]{1,0:T(8,128)(2,1)S(1)} %collective-permute-done.24.refs_1_, bf16[256,256]{1,0:T(8,128)(2,1)S(1)} %collective-permute-done.25.refs_2_, bf16[256,256]{1,0:T(8,128)(2,1)S(1)} %collective-permute-done.26.refs_3_, ...), custom_call_target="tpu_custom_call" | custom-call | tf_op jit(solution)/shard_map/pallas_call | solution.py:385
  134.7 9.0 %all-to-all-start.2 = ((bf16[32,8,1024]{2,1,0:T(8,128)(2,1)}), bf16[32,8,1024]{2,1,0:T(8,128)(2,1)S(1)}, u32[]{:S(2)}, u32[]{:S(2)}) async-start(bf16[32,8,1024]{2,1,0:T(8,128)(2,1)} %bitcast.29), calls=%async_computation.2 | async-start | bytes 1048576 | tf_op jit(solution)/shard_map/all_to_all | solution.py:409
  145.4 3.5 %collective-permute-start.12 = (bf16[16,4096]{1,0:T(8,128)(2,1)S(1)}, bf16[16,4096]{1,0:T(8,128)(2,1)S(1)}, u32[]{:S(2)}, u32[]{:S(2)}) collective-permute-start(bf16[16,4096]{1,0:T(8,128)(2,1)S(1)} %get-tuple-element.44), channel_id=1, source_target_pairs={{0,4},{2,6},{4,0},{6,2},{1,5},{3,7},{5,1},{7,3},{8,12},{10,14},{12... | collective-permute-start | bytes 393224 | tf_op jit(solution)/shard_map/ppermute | solution.py:170
  151.0 8.6 %all-to-all-done.2 = bf16[32,8,1024]{2,1,0:T(8,128)(2,1)S(1)} async-done(((bf16[32,8,1024]{2,1,0:T(8,128)(2,1)}), bf16[32,8,1024]{2,1,0:T(8,128)(2,1)S(1)}, u32[]{:S(2)}, u32[]{:S(2)}) %all-to-all-start.2) | async-done | bytes 524320 | tf_op jit(solution)/shard_map/all_to_all | solution.py:409
  163.6 3.7 %collective-permute-start.28 = (bf16[2,16,1024]{2,1,0:T(8,128)(2,1)}, bf16[2,16,1024]{2,1,0:T(8,128)(2,1)S(1)}, u32[]{:S(2)}, u32[]{:S(2)}) collective-permute-start(bf16[2,16,1024]{2,1,0:T(8,128)(2,1)} %get-tuple-element.40), channel_id=1, source_target_pairs={{0,4},{2,6},{4,0},{6,2},{1,5},{3,7},{5,1},{7,3},{8,12},{10,14},{12... | collective-permute-start | bytes 196616 | tf_op jit(solution)/shard_map/ppermute | solution.py:170
  (115 shorter events, 54.7 us)
Async XLA Ops:
  2.6 14.7 %collective-permute-start = (bf16[208,128]{1,0:T(8,128)(2,1)}, bf16[208,128]{1,0:T(8,128)(2,1)S(1)}, u32[]{:S(2)}, u32[]{:S(2)}) collective-permute-start(bf16[208,128]{1,0:T(8,128)(2,1)} %get-tuple-element.23), channel_id=1, source_target_pairs={{0,32},{32,64},{64,96},{96,128},{128,160},{160,192},{192,224},{224... | collective-permute-start | bytes 159752 | tf_op jit(solution)/shard_map/ppermute | solution.py:170
  4.5 15.5 %collective-permute-start.1 = (bf16[208,128]{1,0:T(8,128)(2,1)}, bf16[208,128]{1,0:T(8,128)(2,1)S(1)}, u32[]{:S(2)}, u32[]{:S(2)}) collective-permute-start(bf16[208,128]{1,0:T(8,128)(2,1)} %get-tuple-element.24), channel_id=1, source_target_pairs={{0,64},{32,96},{64,128},{96,160},{128,192},{160,224},{192,0},{224,... | collective-permute-start | bytes 159752 | tf_op jit(solution)/shard_map/ppermute | solution.py:170
  7.8 13.2 %collective-permute-start.2 = (bf16[208,128]{1,0:T(8,128)(2,1)}, bf16[208,128]{1,0:T(8,128)(2,1)S(1)}, u32[]{:S(2)}, u32[]{:S(2)}) collective-permute-start(bf16[208,128]{1,0:T(8,128)(2,1)} %get-tuple-element.25), channel_id=1, source_target_pairs={{0,96},{32,128},{64,160},{96,192},{128,224},{160,0},{192,32},{224,... | collective-permute-start | bytes 159752 | tf_op jit(solution)/shard_map/ppermute | solution.py:170
  11.9 9.2 %collective-permute-start.3 = (bf16[208,128]{1,0:T(8,128)(2,1)}, bf16[208,128]{1,0:T(8,128)(2,1)S(1)}, u32[]{:S(2)}, u32[]{:S(2)}) collective-permute-start(bf16[208,128]{1,0:T(8,128)(2,1)} %get-tuple-element.26), channel_id=1, source_target_pairs={{0,128},{32,160},{64,192},{96,224},{128,0},{160,32},{192,64},{224,... | collective-permute-start | bytes 159752 | tf_op jit(solution)/shard_map/ppermute | solution.py:170
  12.4 12.3 %collective-permute-start.4 = (bf16[208,128]{1,0:T(8,128)(2,1)}, bf16[208,128]{1,0:T(8,128)(2,1)S(1)}, u32[]{:S(2)}, u32[]{:S(2)}) collective-permute-start(bf16[208,128]{1,0:T(8,128)(2,1)} %get-tuple-element.27), channel_id=1, source_target_pairs={{0,160},{32,192},{64,224},{96,0},{128,32},{160,64},{192,96},{224,1... | collective-permute-start | bytes 159752 | tf_op jit(solution)/shard_map/ppermute | solution.py:170
  27.9 13.2 %collective-permute-start.7 = (bf16[8,144,128]{2,1,0:T(8,128)(2,1)}, bf16[8,144,128]{2,1,0:T(8,128)(2,1)S(1)}, u32[]{:S(2)}, u32[]{:S(2)}) collective-permute-start(bf16[8,144,128]{2,1,0:T(8,128)(2,1)} %shard_map.123), channel_id=1, source_target_pairs={{0,8},{8,16},{16,24},{24,0},{1,9},{9,17},{17,25},{25,1},{2,10},{10... | collective-permute-start | bytes 884744 | tf_op jit(solution)/shard_map/ppermute | solution.py:170
  29.4 13.0 %collective-permute-start.8 = (bf16[8,144,128]{2,1,0:T(8,128)(2,1)}, bf16[8,144,128]{2,1,0:T(8,128)(2,1)}, u32[]{:S(2)}, u32[]{:S(2)}) collective-permute-start(bf16[8,144,128]{2,1,0:T(8,128)(2,1)} %shard_map.123), channel_id=1, source_target_pairs={{0,16},{8,24},{16,0},{24,8},{1,17},{9,25},{17,1},{25,9},{2,18},{10... | collective-permute-start | bytes 884744 | tf_op jit(solution)/shard_map/ppermute | solution.py:170
  30.5 14.3 %collective-permute-start.9 = (bf16[8,144,128]{2,1,0:T(8,128)(2,1)}, bf16[8,144,128]{2,1,0:T(8,128)(2,1)}, u32[]{:S(2)}, u32[]{:S(2)}) collective-permute-start(bf16[8,144,128]{2,1,0:T(8,128)(2,1)} %shard_map.123), channel_id=1, source_target_pairs={{0,24},{8,0},{16,8},{24,16},{1,25},{9,1},{17,9},{25,17},{2,26},{10... | collective-permute-start | bytes 884744 | tf_op jit(solution)/shard_map/ppermute | solution.py:170
  36.5 47.5 %collective-permute-start.14 = (bf16[3072,128]{1,0:T(8,128)(2,1)}, bf16[3072,128]{1,0:T(8,128)(2,1)S(1)}, u32[]{:S(2)}, u32[]{:S(2)}) collective-permute-start(bf16[3072,128]{1,0:T(8,128)(2,1)} %get-tuple-element.31), channel_id=1, source_target_pairs={{0,2},{2,4},{4,6},{6,0},{1,3},{3,5},{5,7},{7,1},{8,10},{10,12},{12... | collective-permute-start | bytes 2359304 | tf_op jit(solution)/shard_map/ppermute | solution.py:170
  38.2 46.4 %collective-permute-start.15 = (bf16[3072,128]{1,0:T(8,128)(2,1)}, bf16[3072,128]{1,0:T(8,128)(2,1)S(1)}, u32[]{:S(2)}, u32[]{:S(2)}) collective-permute-start(bf16[3072,128]{1,0:T(8,128)(2,1)} %get-tuple-element.32), channel_id=1, source_target_pairs={{0,4},{2,6},{4,0},{6,2},{1,5},{3,7},{5,1},{7,3},{8,12},{10,14},{12... | collective-permute-start | bytes 2359304 | tf_op jit(solution)/shard_map/ppermute | solution.py:170
  41.1 43.6 %collective-permute-start.16 = (bf16[3072,128]{1,0:T(8,128)(2,1)}, bf16[3072,128]{1,0:T(8,128)(2,1)S(1)}, u32[]{:S(2)}, u32[]{:S(2)}) collective-permute-start(bf16[3072,128]{1,0:T(8,128)(2,1)} %get-tuple-element.33), channel_id=1, source_target_pairs={{0,6},{2,0},{4,2},{6,4},{1,7},{3,1},{5,3},{7,5},{8,14},{10,8},{12,... | collective-permute-start | bytes 2359304 | tf_op jit(solution)/shard_map/ppermute | solution.py:170
  66.4 12.6 %all-to-all-start = ((bf16[8,64,128]{2,1,0:T(8,128)(2,1)}), bf16[8,64,128]{2,1,0:T(8,128)(2,1)S(1)}, u32[]{:S(2)}, u32[]{:S(2)}) async-start(bf16[8,64,128]{2,1,0:T(8,128)(2,1)} %shard_map.124), calls=%async_computation | async-start | bytes 262144 | tf_op jit(solution)/shard_map/all_to_all | solution.py:181
  79.0 20.8 %all-to-all-start.1 = ((bf16[32,8,1024]{2,1,0:T(8,128)(2,1)}), bf16[32,8,1024]{2,1,0:T(8,128)(2,1)}, u32[]{:S(2)}, u32[]{:S(2)}) async-start(bf16[32,8,1024]{2,1,0:T(8,128)(2,1)} %bitcast.33), calls=%async_computation.1 | async-start | bytes 1048576 | tf_op jit(solution)/shard_map/all_to_all | solution.py:402
  84.0 15.8 %collective-permute-start.18 = (bf16[3072,128]{1,0:T(8,128)(2,1)S(1)}, bf16[3072,128]{1,0:T(8,128)(2,1)}, u32[]{:S(2)}, u32[]{:S(2)}) collective-permute-start(bf16[3072,128]{1,0:T(8,128)(2,1)S(1)} %collective-permute-done.14.refs_2_.refs_5_), channel_id=1, source_target_pairs={{0,1},{1,0},{2,3},{3,2},{4,5},{5,4},{6,7},{7,6},{8,9},{9,8},{10,11... | collective-permute-start | bytes 2359304 | tf_op jit(solution)/shard_map/ppermute | solution.py:170
  84.5 15.3 %collective-permute-start.19 = (bf16[3072,128]{1,0:T(8,128)(2,1)S(1)}, bf16[3072,128]{1,0:T(8,128)(2,1)}, u32[]{:S(2)}, u32[]{:S(2)}) collective-permute-start(bf16[3072,128]{1,0:T(8,128)(2,1)S(1)} %collective-permute-done.15.refs_3_.refs_6_), channel_id=1, source_target_pairs={{0,1},{1,0},{2,3},{3,2},{4,5},{5,4},{6,7},{7,6},{8,9},{9,8},{10,11... | collective-permute-start | bytes 2359304 | tf_op jit(solution)/shard_map/ppermute | solution.py:170
  84.7 15.2 %collective-permute-start.20 = (bf16[3072,128]{1,0:T(8,128)(2,1)S(1)}, bf16[3072,128]{1,0:T(8,128)(2,1)}, u32[]{:S(2)}, u32[]{:S(2)}) collective-permute-start(bf16[3072,128]{1,0:T(8,128)(2,1)S(1)} %collective-permute-done.16.refs_4_.refs_7_), channel_id=1, source_target_pairs={{0,1},{1,0},{2,3},{3,2},{4,5},{5,4},{6,7},{7,6},{8,9},{9,8},{10,11... | collective-permute-start | bytes 2359304 | tf_op jit(solution)/shard_map/ppermute | solution.py:170
  89.8 53.9 %collective-permute-start.10 = (bf16[4,16,4096]{2,1,0:T(8,128)(2,1)}, bf16[4,16,4096]{2,1,0:T(8,128)(2,1)}, u32[]{:S(2)}, u32[]{:S(2)}) collective-permute-start(bf16[4,16,4096]{2,1,0:T(8,128)(2,1)} %dynamic-slice_bitcast_fusion), channel_id=1, source_target_pairs={{0,1},{1,0},{2,3},{3,2},{4,5},{5,4},{6,7},{7,6},{8,9},{9,8},{10,11... | collective-permute-start | bytes 1572872 | tf_op jit(solution)/shard_map/ppermute | solution.py:170
  103.9 11.2 %collective-permute-start.21 = (bf16[256,512]{1,0:T(8,128)(2,1)S(1)}, bf16[256,512]{1,0:T(8,128)(2,1)S(1)}, u32[]{:S(2)}, u32[]{:S(2)}) collective-permute-start(bf16[256,512]{1,0:T(8,128)(2,1)S(1)} %get-tuple-element.35), channel_id=1, source_target_pairs={{0,6},{2,0},{4,2},{6,4},{1,7},{3,1},{5,3},{7,5},{8,14},{10,8},{12,... | collective-permute-start | bytes 786440 | tf_op jit(solution)/shard_map/ppermute | solution.py:170
  106.9 9.3 %collective-permute-start.22 = (bf16[256,512]{1,0:T(8,128)(2,1)S(1)}, bf16[256,512]{1,0:T(8,128)(2,1)S(1)}, u32[]{:S(2)}, u32[]{:S(2)}) collective-permute-start(bf16[256,512]{1,0:T(8,128)(2,1)S(1)} %get-tuple-element.36), channel_id=1, source_target_pairs={{0,4},{2,6},{4,0},{6,2},{1,5},{3,7},{5,1},{7,3},{8,12},{10,14},{12... | collective-permute-start | bytes 786440 | tf_op jit(solution)/shard_map/ppermute | solution.py:170
  107.6 11.3 %collective-permute-start.23 = (bf16[256,512]{1,0:T(8,128)(2,1)S(1)}, bf16[256,512]{1,0:T(8,128)(2,1)S(1)}, u32[]{:S(2)}, u32[]{:S(2)}) collective-permute-start(bf16[256,512]{1,0:T(8,128)(2,1)S(1)} %get-tuple-element.37), channel_id=1, source_target_pairs={{0,2},{2,4},{4,6},{6,0},{1,3},{3,5},{5,7},{7,1},{8,10},{10,12},{12... | collective-permute-start | bytes 786440 | tf_op jit(solution)/shard_map/ppermute | solution.py:170
  134.7 25.0 %all-to-all-start.2 = ((bf16[32,8,1024]{2,1,0:T(8,128)(2,1)}), bf16[32,8,1024]{2,1,0:T(8,128)(2,1)S(1)}, u32[]{:S(2)}, u32[]{:S(2)}) async-start(bf16[32,8,1024]{2,1,0:T(8,128)(2,1)} %bitcast.29), calls=%async_computation.2 | async-start | bytes 1048576 | tf_op jit(solution)/shard_map/all_to_all | solution.py:409
  145.1 22.2 %collective-permute-start.11 = (bf16[16,4096]{1,0:T(8,128)(2,1)S(1)}, bf16[16,4096]{1,0:T(8,128)(2,1)S(1)}, u32[]{:S(2)}, u32[]{:S(2)}) collective-permute-start(bf16[16,4096]{1,0:T(8,128)(2,1)S(1)} %get-tuple-element.42), channel_id=1, source_target_pairs={{0,2},{2,4},{4,6},{6,0},{1,3},{3,5},{5,7},{7,1},{8,10},{10,12},{12... | collective-permute-start | bytes 393224 | tf_op jit(solution)/shard_map/ppermute | solution.py:170
  145.4 21.9 %collective-permute-start.12 = (bf16[16,4096]{1,0:T(8,128)(2,1)S(1)}, bf16[16,4096]{1,0:T(8,128)(2,1)S(1)}, u32[]{:S(2)}, u32[]{:S(2)}) collective-permute-start(bf16[16,4096]{1,0:T(8,128)(2,1)S(1)} %get-tuple-element.44), channel_id=1, source_target_pairs={{0,4},{2,6},{4,0},{6,2},{1,5},{3,7},{5,1},{7,3},{8,12},{10,14},{12... | collective-permute-start | bytes 393224 | tf_op jit(solution)/shard_map/ppermute | solution.py:170
  149.0 18.4 %collective-permute-start.13 = (bf16[16,4096]{1,0:T(8,128)(2,1)S(1)}, bf16[16,4096]{1,0:T(8,128)(2,1)S(1)}, u32[]{:S(2)}, u32[]{:S(2)}) collective-permute-start(bf16[16,4096]{1,0:T(8,128)(2,1)S(1)} %get-tuple-element.43), channel_id=1, source_target_pairs={{0,6},{2,0},{4,2},{6,4},{1,7},{3,1},{5,3},{7,5},{8,14},{10,8},{12,... | collective-permute-start | bytes 393224 | tf_op jit(solution)/shard_map/ppermute | solution.py:170
  (37 other events, 174.6 us)

commit v2 on v1

--- a/solution.py
+++ b/solution.py
@@ -9,6 +9,7 @@
 HEAD = 64
 Z, X, Y, C = 8, 4, 4, 2
 BF = jnp.bfloat16
+MIB = 1024 * 1024
 F32 = jnp.float32
 
 STEPS = (
@@ -118,7 +119,7 @@
             pltpu.VMEM((8, 128, HEAD), F32),
             pltpu.SMEM((len(STEPS), 8), jnp.int32),
         ],
-        compiler_params=pltpu.CompilerParams(vmem_limit_bytes=32 * 1024 * 1024),
+        compiler_params=pltpu.CompilerParams(vmem_limit_bytes=14 * MIB),
         cost_estimate=pl.CostEstimate(flops=4_000_000_000, transcendentals=7_000_000, bytes_accessed=2_000_000),
     )(*arrived, *pieces)
 
@@ -257,6 +258,7 @@
         in_specs=[VMEM, VMEM],
         out_specs=[VMEM] * Y,
         scratch_shapes=[pltpu.VMEM((2, 128, width), BF)],
+        compiler_params=pltpu.CompilerParams(vmem_limit_bytes=5 * MIB),
     )(ids, rows)
 
 
@@ -290,6 +292,7 @@
         out_shape=jax.ShapeDtypeStruct((16, Y * picked[0].shape[2]), BF),
         in_specs=[VMEM] * 5,
         out_specs=VMEM,
+        compiler_params=pltpu.CompilerParams(vmem_limit_bytes=4 * MIB),
     )(*picked, weights)
 
 
@@ -344,7 +347,7 @@
         out_shape=[jax.ShapeDtypeStruct((rows.shape[0], 512), F32), sent, sent, sent],
         in_specs=[VMEM] * (1 + 2 * Y),
         out_specs=[VMEM] * Y,
-        compiler_params=pltpu.CompilerParams(vmem_limit_bytes=32 * 1024 * 1024),
+        compiler_params=pltpu.CompilerParams(vmem_limit_bytes=16 * MIB),
     )(rows, *ours, *theirs)
 
 
@@ -363,6 +366,7 @@
         out_shape=jax.ShapeDtypeStruct((parts[0].shape[0], 256), BF),
         in_specs=[VMEM] * 4,
         out_specs=VMEM,
+        compiler_params=pltpu.CompilerParams(vmem_limit_bytes=5 * MIB),
     )(*parts)
 
 
@@ -387,7 +391,7 @@
         out_shape=jax.ShapeDtypeStruct((rows, width), BF),
         in_specs=[VMEM] * (3 * Y),
         out_specs=VMEM,
-        compiler_params=pltpu.CompilerParams(vmem_limit_bytes=32 * 1024 * 1024),
+        compiler_params=pltpu.CompilerParams(vmem_limit_bytes=16 * MIB),
     )(*units, *ours, *theirs)
 
 

time: 175 us -> 167 us (0.954)
  Pallas kernels: 38.6 us -> 34 us
  local copies, waits for them, and re-layouts: 14.3 us -> 11.2 us
    unnamed x57 -> x43, local copies, waits for them, and re-layouts: 13.4 us -> 10.3 us
    pallas_call x1, Pallas kernels: 2.1 us -> 0.18 us  [hidden_units(): pl.pallas_call(hidden_kernel, out_shape=jax.ShapeDtypeStruct((parts[0].sh...]
  transfers between devices with their start and end apart: 33 -> 33, of which waited for: 14 -> 14; matrix products, arithmetic and copies ran while one was open for 4% -> 4% of each run, Pallas kernels for 19% -> 18%
where the time goes in v2:
time: 167 us; the launch traced here: 166 us
  starting transfers between devices  64.4 us (39%)
  waiting for transfers between devices  50.9 us (30%)
  Pallas kernels  34 us (20%)
  local copies, waits for them, and re-layouts  11.2 us (7%)
  matrix products  2.93 us (2%)
  other arithmetic  2.06 us (1%)
    ppermute x30, starting transfers between devices, shifted(): lax.ppermute(value, axis, [(i, (i + by) % size) for i in range(size)])  46.9 us
    ppermute x30, waiting for transfers between devices, shifted(): lax.ppermute(value, axis, [(i, (i + by) % size) for i in range(size)])  26.1 us
    pallas_call x1, Pallas kernels, attend(): pl.pallas_call(attend_kernel, out_shape=jax.ShapeDtypeStruct((8, HEAD, 12...  15.1 us
    unnamed x43, local copies, waits for them, and re-layouts  10.3 us
    all_to_all x1, waiting for transfers between devices, experts(): lax.all_to_all(outgoing, ep, split_axis=0, concat_axis=0, tiled=True)  9.85 us
    all_to_all x1, starting transfers between devices, experts(): lax.all_to_all(result.reshape(Z * X, 8, width), ep, split_axis=0, concat_...  9.05 us
    all_to_all x1, waiting for transfers between devices, experts(): lax.all_to_all(result.reshape(Z * X, 8, width), ep, split_axis=0, concat_...  8.59 us
    all_to_all x1, waiting for transfers between devices, mixer(): attended = lax.all_to_all(out, 'z', split_axis=0, concat_axis=0, tiled=True)  6.33 us
  transfers between devices with their start and end apart: 33, of which 14 were waited for; matrix products, arithmetic and copies ran while one was open for 4% of the time, Pallas kernels for 18%

profile of v2, /device:TPU:2, one launch (start us, length us, event | category | flops | bytes accessed | tf_op | source)
XLA Modules:
  0.0 166.3 jit_solution(5488887300272213721)
XLA Ops:
  4.6 3.3 %collective-permute-start.1 = (bf16[208,128]{1,0:T(8,128)(2,1)}, bf16[208,128]{1,0:T(8,128)(2,1)S(1)}, u32[]{:S(2)}, u32[]{:S(2)}) collective-permute-start(bf16[208,128]{1,0:T(8,128)(2,1)} %get-tuple-element.24), channel_id=1, source_target_pairs={{0,64},{32,96},{64,128},{96,160},{128,192},{160,224},{192,0},{224,... | collective-permute-start | bytes 159752 | tf_op jit(solution)/shard_map/ppermute | solution.py:171
  7.8 4.0 %collective-permute-start.2 = (bf16[208,128]{1,0:T(8,128)(2,1)}, bf16[208,128]{1,0:T(8,128)(2,1)S(1)}, u32[]{:S(2)}, u32[]{:S(2)}) collective-permute-start(bf16[208,128]{1,0:T(8,128)(2,1)} %get-tuple-element.25), channel_id=1, source_target_pairs={{0,96},{32,128},{64,160},{96,192},{128,224},{160,0},{192,32},{224,... | collective-permute-start | bytes 159752 | tf_op jit(solution)/shard_map/ppermute | solution.py:171
  12.4 4.9 %collective-permute-start.4 = (bf16[208,128]{1,0:T(8,128)(2,1)}, bf16[208,128]{1,0:T(8,128)(2,1)S(1)}, u32[]{:S(2)}, u32[]{:S(2)}) collective-permute-start(bf16[208,128]{1,0:T(8,128)(2,1)} %get-tuple-element.27), channel_id=1, source_target_pairs={{0,160},{32,192},{64,224},{96,0},{128,32},{160,64},{192,96},{224,1... | collective-permute-start | bytes 159752 | tf_op jit(solution)/shard_map/ppermute | solution.py:171
  17.4 2.7 %collective-permute-start.5 = (bf16[208,128]{1,0:T(8,128)(2,1)}, bf16[208,128]{1,0:T(8,128)(2,1)S(1)}, u32[]{:S(2)}, u32[]{:S(2)}) collective-permute-start(bf16[208,128]{1,0:T(8,128)(2,1)} %get-tuple-element.28), channel_id=1, source_target_pairs={{0,192},{32,224},{64,0},{96,32},{128,64},{160,96},{192,128},{224,1... | collective-permute-start | bytes 159752 | tf_op jit(solution)/shard_map/ppermute | solution.py:171
  21.1 3.7 %collective-permute-done.4.refs_5_ = bf16[208,128]{1,0:T(8,128)(2,1)S(1)} collective-permute-done((bf16[208,128]{1,0:T(8,128)(2,1)}, bf16[208,128]{1,0:T(8,128)(2,1)S(1)}, u32[]{:S(2)}, u32[]{:S(2)}) %collective-permute-start.4) | collective-permute-done | bytes 53280 | tf_op jit(solution)/shard_map/ppermute | solution.py:171
  32.7 3.8 %shard_map.126 = (bf16[3072,128]{1,0:T(8,128)(2,1)}, bf16[3072,128]{1,0:T(8,128)(2,1)}, bf16[3072,128]{1,0:T(8,128)(2,1)}, bf16[3072,128]{1,0:T(8,128)(2,1)}) custom-call(bf16[4096,128]{1,0:T(8,128)(2,1)} %bitcast.36, bf16[4096,128]{1,0:T(8,128)(2,1)} %bitcast.37, bf16[128,4096]{1,0:T(8,128)(2,1)} %bitcast.38), custom_call_target="tpu_custom_call" | custom-call | tf_op jit(solution)/shard_map/pallas_call | solution.py:323
  38.2 2.9 %collective-permute-start.15 = (bf16[3072,128]{1,0:T(8,128)(2,1)}, bf16[3072,128]{1,0:T(8,128)(2,1)S(1)}, u32[]{:S(2)}, u32[]{:S(2)}) collective-permute-start(bf16[3072,128]{1,0:T(8,128)(2,1)} %get-tuple-element.32), channel_id=1, source_target_pairs={{0,4},{2,6},{4,0},{6,2},{1,5},{3,7},{5,1},{7,3},{8,12},{10,14},{12... | collective-permute-start | bytes 2359304 | tf_op jit(solution)/shard_map/ppermute | solution.py:171
  51.3 15.1 %shard_map.124 = bf16[8,64,128]{2,1,0:T(8,128)(2,1)} custom-call(bf16[208,128]{1,0:T(8,128)(2,1)S(1)} %copy-done.3, bf16[208,128]{1,0:T(8,128)(2,1)S(1)} %copy-done.5, bf16[208,128]{1,0:T(8,128)(2,1)S(1)} %copy-done.7, bf16[208,128]{1,0:T(8,128)(2,1)S(1)} %copy-done.9, bf16[208,128]{1,0:T(8,128)(2,1)S(1)} %copy-done.11, bf16[208,128]{1,0:T(8,128)(2,1)S(1)} %copy-done.13, ...), custom_call_target="tpu_custom_call" | custom-call | flops 4000000000 | bytes 2000000 | tf_op jit(solution)/shard_map/pallas_call | solution.py:109
  66.4 3.6 %all-to-all-start = ((bf16[8,64,128]{2,1,0:T(8,128)(2,1)}), bf16[8,64,128]{2,1,0:T(8,128)(2,1)S(1)}, u32[]{:S(2)}, u32[]{:S(2)}) async-start(bf16[8,64,128]{2,1,0:T(8,128)(2,1)} %shard_map.124), calls=%async_computation | async-start | bytes 262144 | tf_op jit(solution)/shard_map/all_to_all | solution.py:182
  70.0 2.7 %shard_map.125 = bf16[256,1024]{1,0:T(8,128)(2,1)} custom-call(s32[2,128]{1,0:T(2,128)} %bitcast.31, bf16[128,4096]{1,0:T(8,128)(2,1)} %rows_ref.1), custom_call_target="tpu_custom_call" | custom-call | tf_op jit(solution)/shard_map/pallas_call | solution.py:234
  72.7 6.3 %all-to-all-done = bf16[8,64,128]{2,1,0:T(8,128)(2,1)S(1)} async-done(((bf16[8,64,128]{2,1,0:T(8,128)(2,1)}), bf16[8,64,128]{2,1,0:T(8,128)(2,1)S(1)}, u32[]{:S(2)}, u32[]{:S(2)}) %all-to-all-start) | async-done | bytes 131104 | tf_op jit(solution)/shard_map/all_to_all | solution.py:182
  79.0 4.9 %all-to-all-start.1 = ((bf16[32,8,1024]{2,1,0:T(8,128)(2,1)}), bf16[32,8,1024]{2,1,0:T(8,128)(2,1)}, u32[]{:S(2)}, u32[]{:S(2)}) async-start(bf16[32,8,1024]{2,1,0:T(8,128)(2,1)} %bitcast.35), calls=%async_computation.1 | async-start | bytes 1048576 | tf_op jit(solution)/shard_map/all_to_all | solution.py:406
  85.1 2.9 %convolution_convert_fusion = bf16[128,4096]{1,0:T(8,128)(2,1)S(1)} fusion(bf16[512,128]{1,0:T(8,128)(2,1)S(1)} %bitcast.39, bf16[512,4096]{1,0:T(8,128)(2,1)} %param.15), kind=kOutput, calls=%fused_computation | convolution fusion | flops 537395200 | bytes 5373952 | tf_op jit(solution)/shard_map/dot_general | solution.py:184
  90.0 9.8 %all-to-all-done.1 = bf16[32,8,1024]{2,1,0:T(8,128)(2,1)} async-done(((bf16[32,8,1024]{2,1,0:T(8,128)(2,1)}), bf16[32,8,1024]{2,1,0:T(8,128)(2,1)}, u32[]{:S(2)}, u32[]{:S(2)}) %all-to-all-start.1) | async-done | bytes 524320 | tf_op jit(solution)/shard_map/all_to_all | solution.py:406
  99.8 3.3 %shard_map.127 = (f32[256,512]{1,0:T(8,128)S(1)}, bf16[256,512]{1,0:T(8,128)(2,1)S(1)}, bf16[256,512]{1,0:T(8,128)(2,1)S(1)}, bf16[256,512]{1,0:T(8,128)(2,1)S(1)}) custom-call(bf16[256,1024]{1,0:T(8,128)(2,1)} %bitcast.11.refs_0_, bf16[3072,128]{1,0:T(8,128)(2,1)S(1)} %copy-done, bf16[3072,128]{1,0:T(8,128)(2,1)S(1)} %collective-permute-done.14.refs_2_.refs_5_, ...), custom_call_target="tpu_custom_call" | custom-call | tf_op jit(solution)/shard_map/pallas_call | solution.py:345
  103.1 3.1 %collective-permute-start.21 = (bf16[256,512]{1,0:T(8,128)(2,1)S(1)}, bf16[256,512]{1,0:T(8,128)(2,1)S(1)}, u32[]{:S(2)}, u32[]{:S(2)}) collective-permute-start(bf16[256,512]{1,0:T(8,128)(2,1)S(1)} %get-tuple-element.35), channel_id=1, source_target_pairs={{0,6},{2,0},{4,2},{6,4},{1,7},{3,1},{5,3},{7,5},{8,14},{10,8},{12,... | collective-permute-start | bytes 786440 | tf_op jit(solution)/shard_map/ppermute | solution.py:171
  107.8 6.6 %collective-permute-done.21.p1_ref = bf16[256,512]{1,0:T(8,128)(2,1)S(1)} collective-permute-done((bf16[256,512]{1,0:T(8,128)(2,1)S(1)}, bf16[256,512]{1,0:T(8,128)(2,1)S(1)}, u32[]{:S(2)}, u32[]{:S(2)}) %collective-permute-start.21) | collective-permute-done | bytes 262176 | tf_op jit(solution)/shard_map/ppermute | solution.py:171
  115.5 2.7 %collective-permute-done.23.p3_ref = bf16[256,512]{1,0:T(8,128)(2,1)S(1)} collective-permute-done((bf16[256,512]{1,0:T(8,128)(2,1)S(1)}, bf16[256,512]{1,0:T(8,128)(2,1)S(1)}, u32[]{:S(2)}, u32[]{:S(2)}) %collective-permute-start.23) | collective-permute-done | bytes 262176 | tf_op jit(solution)/shard_map/ppermute | solution.py:171
  121.7 4.6 %collective-permute-done.24.refs_1_ = bf16[256,256]{1,0:T(8,128)(2,1)S(1)} collective-permute-done((bf16[256,256]{1,0:T(8,128)(2,1)S(1)}, bf16[256,256]{1,0:T(8,128)(2,1)S(1)}, u32[]{:S(2)}, u32[]{:S(2)}) %collective-permute-start.24) | collective-permute-done | bytes 131104 | tf_op jit(solution)/shard_map/ppermute | solution.py:171
  127.0 2.6 %shard_map.129 = bf16[256,1024]{1,0:T(8,128)(2,1)S(1)} custom-call(bf16[256,256]{1,0:T(8,128)(2,1)S(1)} %shard_map.128.refs_0_, bf16[256,256]{1,0:T(8,128)(2,1)S(1)} %collective-permute-done.24.refs_1_, bf16[256,256]{1,0:T(8,128)(2,1)S(1)} %collective-permute-done.25.refs_2_, bf16[256,256]{1,0:T(8,128)(2,1)} %collective-permute-done.26.refs_3_, ...), custom_call_target="tpu_custom_call" | custom-call | tf_op jit(solution)/shard_map/pallas_call | solution.py:389
  130.4 9.1 %all-to-all-start.2 = ((bf16[32,8,1024]{2,1,0:T(8,128)(2,1)}), bf16[32,8,1024]{2,1,0:T(8,128)(2,1)S(1)}, u32[]{:S(2)}, u32[]{:S(2)}) async-start(bf16[32,8,1024]{2,1,0:T(8,128)(2,1)} %bitcast.29), calls=%async_computation.2 | async-start | bytes 1048576 | tf_op jit(solution)/shard_map/all_to_all | solution.py:413
  141.2 3.6 %collective-permute-start.12 = (bf16[16,4096]{1,0:T(8,128)(2,1)S(1)}, bf16[16,4096]{1,0:T(8,128)(2,1)S(1)}, u32[]{:S(2)}, u32[]{:S(2)}) collective-permute-start(bf16[16,4096]{1,0:T(8,128)(2,1)S(1)} %get-tuple-element.44), channel_id=1, source_target_pairs={{0,4},{2,6},{4,0},{6,2},{1,5},{3,7},{5,1},{7,3},{8,12},{10,14},{12... | collective-permute-start | bytes 393224 | tf_op jit(solution)/shard_map/ppermute | solution.py:171
  146.8 8.6 %all-to-all-done.2 = bf16[32,8,1024]{2,1,0:T(8,128)(2,1)S(1)} async-done(((bf16[32,8,1024]{2,1,0:T(8,128)(2,1)}), bf16[32,8,1024]{2,1,0:T(8,128)(2,1)S(1)}, u32[]{:S(2)}, u32[]{:S(2)}) %all-to-all-start.2) | async-done | bytes 524320 | tf_op jit(solution)/shard_map/all_to_all | solution.py:413
  156.9 3.7 %collective-permute-start.28 = (bf16[2,16,1024]{2,1,0:T(8,128)(2,1)S(1)}, bf16[2,16,1024]{2,1,0:T(8,128)(2,1)S(1)}, u32[]{:S(2)}, u32[]{:S(2)}) collective-permute-start(bf16[2,16,1024]{2,1,0:T(8,128)(2,1)S(1)} %get-tuple-element.40), channel_id=1, source_target_pairs={{0,4},{2,6},{4,0},{6,2},{1,5},{3,7},{5,1},{7,3},{8,12},{10,14},{12... | collective-permute-start | bytes 196616 | tf_op jit(solution)/shard_map/ppermute | solution.py:171
  (101 shorter events, 46.9 us)
Async XLA Ops:
  2.6 14.7 %collective-permute-start = (bf16[208,128]{1,0:T(8,128)(2,1)}, bf16[208,128]{1,0:T(8,128)(2,1)S(1)}, u32[]{:S(2)}, u32[]{:S(2)}) collective-permute-start(bf16[208,128]{1,0:T(8,128)(2,1)} %get-tuple-element.23), channel_id=1, source_target_pairs={{0,32},{32,64},{64,96},{96,128},{128,160},{160,192},{192,224},{224... | collective-permute-start | bytes 159752 | tf_op jit(solution)/shard_map/ppermute | solution.py:171
  4.6 15.5 %collective-permute-start.1 = (bf16[208,128]{1,0:T(8,128)(2,1)}, bf16[208,128]{1,0:T(8,128)(2,1)S(1)}, u32[]{:S(2)}, u32[]{:S(2)}) collective-permute-start(bf16[208,128]{1,0:T(8,128)(2,1)} %get-tuple-element.24), channel_id=1, source_target_pairs={{0,64},{32,96},{64,128},{96,160},{128,192},{160,224},{192,0},{224,... | collective-permute-start | bytes 159752 | tf_op jit(solution)/shard_map/ppermute | solution.py:171
  7.8 13.2 %collective-permute-start.2 = (bf16[208,128]{1,0:T(8,128)(2,1)}, bf16[208,128]{1,0:T(8,128)(2,1)S(1)}, u32[]{:S(2)}, u32[]{:S(2)}) collective-permute-start(bf16[208,128]{1,0:T(8,128)(2,1)} %get-tuple-element.25), channel_id=1, source_target_pairs={{0,96},{32,128},{64,160},{96,192},{128,224},{160,0},{192,32},{224,... | collective-permute-start | bytes 159752 | tf_op jit(solution)/shard_map/ppermute | solution.py:171
  11.9 9.2 %collective-permute-start.3 = (bf16[208,128]{1,0:T(8,128)(2,1)}, bf16[208,128]{1,0:T(8,128)(2,1)S(1)}, u32[]{:S(2)}, u32[]{:S(2)}) collective-permute-start(bf16[208,128]{1,0:T(8,128)(2,1)} %get-tuple-element.26), channel_id=1, source_target_pairs={{0,128},{32,160},{64,192},{96,224},{128,0},{160,32},{192,64},{224,... | collective-permute-start | bytes 159752 | tf_op jit(solution)/shard_map/ppermute | solution.py:171
  12.4 12.3 %collective-permute-start.4 = (bf16[208,128]{1,0:T(8,128)(2,1)}, bf16[208,128]{1,0:T(8,128)(2,1)S(1)}, u32[]{:S(2)}, u32[]{:S(2)}) collective-permute-start(bf16[208,128]{1,0:T(8,128)(2,1)} %get-tuple-element.27), channel_id=1, source_target_pairs={{0,160},{32,192},{64,224},{96,0},{128,32},{160,64},{192,96},{224,1... | collective-permute-start | bytes 159752 | tf_op jit(solution)/shard_map/ppermute | solution.py:171
  27.9 13.2 %collective-permute-start.7 = (bf16[8,144,128]{2,1,0:T(8,128)(2,1)}, bf16[8,144,128]{2,1,0:T(8,128)(2,1)S(1)}, u32[]{:S(2)}, u32[]{:S(2)}) collective-permute-start(bf16[8,144,128]{2,1,0:T(8,128)(2,1)} %shard_map.123), channel_id=1, source_target_pairs={{0,8},{8,16},{16,24},{24,0},{1,9},{9,17},{17,25},{25,1},{2,10},{10... | collective-permute-start | bytes 884744 | tf_op jit(solution)/shard_map/ppermute | solution.py:171
  29.4 13.0 %collective-permute-start.8 = (bf16[8,144,128]{2,1,0:T(8,128)(2,1)}, bf16[8,144,128]{2,1,0:T(8,128)(2,1)}, u32[]{:S(2)}, u32[]{:S(2)}) collective-permute-start(bf16[8,144,128]{2,1,0:T(8,128)(2,1)} %shard_map.123), channel_id=1, source_target_pairs={{0,16},{8,24},{16,0},{24,8},{1,17},{9,25},{17,1},{25,9},{2,18},{10... | collective-permute-start | bytes 884744 | tf_op jit(solution)/shard_map/ppermute | solution.py:171
  30.5 14.3 %collective-permute-start.9 = (bf16[8,144,128]{2,1,0:T(8,128)(2,1)}, bf16[8,144,128]{2,1,0:T(8,128)(2,1)}, u32[]{:S(2)}, u32[]{:S(2)}) collective-permute-start(bf16[8,144,128]{2,1,0:T(8,128)(2,1)} %shard_map.123), channel_id=1, source_target_pairs={{0,24},{8,0},{16,8},{24,16},{1,25},{9,1},{17,9},{25,17},{2,26},{10... | collective-permute-start | bytes 884744 | tf_op jit(solution)/shard_map/ppermute | solution.py:171
  36.5 47.5 %collective-permute-start.14 = (bf16[3072,128]{1,0:T(8,128)(2,1)}, bf16[3072,128]{1,0:T(8,128)(2,1)S(1)}, u32[]{:S(2)}, u32[]{:S(2)}) collective-permute-start(bf16[3072,128]{1,0:T(8,128)(2,1)} %get-tuple-element.31), channel_id=1, source_target_pairs={{0,2},{2,4},{4,6},{6,0},{1,3},{3,5},{5,7},{7,1},{8,10},{10,12},{12... | collective-permute-start | bytes 2359304 | tf_op jit(solution)/shard_map/ppermute | solution.py:171
  38.2 46.4 %collective-permute-start.15 = (bf16[3072,128]{1,0:T(8,128)(2,1)}, bf16[3072,128]{1,0:T(8,128)(2,1)S(1)}, u32[]{:S(2)}, u32[]{:S(2)}) collective-permute-start(bf16[3072,128]{1,0:T(8,128)(2,1)} %get-tuple-element.32), channel_id=1, source_target_pairs={{0,4},{2,6},{4,0},{6,2},{1,5},{3,7},{5,1},{7,3},{8,12},{10,14},{12... | collective-permute-start | bytes 2359304 | tf_op jit(solution)/shard_map/ppermute | solution.py:171
  41.1 43.6 %collective-permute-start.16 = (bf16[3072,128]{1,0:T(8,128)(2,1)}, bf16[3072,128]{1,0:T(8,128)(2,1)S(1)}, u32[]{:S(2)}, u32[]{:S(2)}) collective-permute-start(bf16[3072,128]{1,0:T(8,128)(2,1)} %get-tuple-element.33), channel_id=1, source_target_pairs={{0,6},{2,0},{4,2},{6,4},{1,7},{3,1},{5,3},{7,5},{8,14},{10,8},{12,... | collective-permute-start | bytes 2359304 | tf_op jit(solution)/shard_map/ppermute | solution.py:171
  66.4 12.7 %all-to-all-start = ((bf16[8,64,128]{2,1,0:T(8,128)(2,1)}), bf16[8,64,128]{2,1,0:T(8,128)(2,1)S(1)}, u32[]{:S(2)}, u32[]{:S(2)}) async-start(bf16[8,64,128]{2,1,0:T(8,128)(2,1)} %shard_map.124), calls=%async_computation | async-start | bytes 262144 | tf_op jit(solution)/shard_map/all_to_all | solution.py:182
  79.0 20.8 %all-to-all-start.1 = ((bf16[32,8,1024]{2,1,0:T(8,128)(2,1)}), bf16[32,8,1024]{2,1,0:T(8,128)(2,1)}, u32[]{:S(2)}, u32[]{:S(2)}) async-start(bf16[32,8,1024]{2,1,0:T(8,128)(2,1)} %bitcast.35), calls=%async_computation.1 | async-start | bytes 1048576 | tf_op jit(solution)/shard_map/all_to_all | solution.py:406
  84.1 15.8 %collective-permute-start.18 = (bf16[3072,128]{1,0:T(8,128)(2,1)S(1)}, bf16[3072,128]{1,0:T(8,128)(2,1)}, u32[]{:S(2)}, u32[]{:S(2)}) collective-permute-start(bf16[3072,128]{1,0:T(8,128)(2,1)S(1)} %collective-permute-done.14.refs_2_.refs_5_), channel_id=1, source_target_pairs={{0,1},{1,0},{2,3},{3,2},{4,5},{5,4},{6,7},{7,6},{8,9},{9,8},{10,11... | collective-permute-start | bytes 2359304 | tf_op jit(solution)/shard_map/ppermute | solution.py:171
  84.5 15.3 %collective-permute-start.19 = (bf16[3072,128]{1,0:T(8,128)(2,1)S(1)}, bf16[3072,128]{1,0:T(8,128)(2,1)}, u32[]{:S(2)}, u32[]{:S(2)}) collective-permute-start(bf16[3072,128]{1,0:T(8,128)(2,1)S(1)} %collective-permute-done.15.refs_3_.refs_6_), channel_id=1, source_target_pairs={{0,1},{1,0},{2,3},{3,2},{4,5},{5,4},{6,7},{7,6},{8,9},{9,8},{10,11... | collective-permute-start | bytes 2359304 | tf_op jit(solution)/shard_map/ppermute | solution.py:171
  84.7 15.2 %collective-permute-start.20 = (bf16[3072,128]{1,0:T(8,128)(2,1)S(1)}, bf16[3072,128]{1,0:T(8,128)(2,1)}, u32[]{:S(2)}, u32[]{:S(2)}) collective-permute-start(bf16[3072,128]{1,0:T(8,128)(2,1)S(1)} %collective-permute-done.16.refs_4_.refs_7_), channel_id=1, source_target_pairs={{0,1},{1,0},{2,3},{3,2},{4,5},{5,4},{6,7},{7,6},{8,9},{9,8},{10,11... | collective-permute-start | bytes 2359304 | tf_op jit(solution)/shard_map/ppermute | solution.py:171
  89.9 49.6 %collective-permute-start.10 = (bf16[4,16,4096]{2,1,0:T(8,128)(2,1)}, bf16[4,16,4096]{2,1,0:T(8,128)(2,1)}, u32[]{:S(2)}, u32[]{:S(2)}) collective-permute-start(bf16[4,16,4096]{2,1,0:T(8,128)(2,1)} %dynamic-slice_bitcast_fusion), channel_id=1, source_target_pairs={{0,1},{1,0},{2,3},{3,2},{4,5},{5,4},{6,7},{7,6},{8,9},{9,8},{10,11... | collective-permute-start | bytes 1572872 | tf_op jit(solution)/shard_map/ppermute | solution.py:171
  103.1 11.3 %collective-permute-start.21 = (bf16[256,512]{1,0:T(8,128)(2,1)S(1)}, bf16[256,512]{1,0:T(8,128)(2,1)S(1)}, u32[]{:S(2)}, u32[]{:S(2)}) collective-permute-start(bf16[256,512]{1,0:T(8,128)(2,1)S(1)} %get-tuple-element.35), channel_id=1, source_target_pairs={{0,6},{2,0},{4,2},{6,4},{1,7},{3,1},{5,3},{7,5},{8,14},{10,8},{12,... | collective-permute-start | bytes 786440 | tf_op jit(solution)/shard_map/ppermute | solution.py:171
  106.2 9.3 %collective-permute-start.22 = (bf16[256,512]{1,0:T(8,128)(2,1)S(1)}, bf16[256,512]{1,0:T(8,128)(2,1)S(1)}, u32[]{:S(2)}, u32[]{:S(2)}) collective-permute-start(bf16[256,512]{1,0:T(8,128)(2,1)S(1)} %get-tuple-element.36), channel_id=1, source_target_pairs={{0,4},{2,6},{4,0},{6,2},{1,5},{3,7},{5,1},{7,3},{8,12},{10,14},{12... | collective-permute-start | bytes 786440 | tf_op jit(solution)/shard_map/ppermute | solution.py:171
  106.8 11.3 %collective-permute-start.23 = (bf16[256,512]{1,0:T(8,128)(2,1)S(1)}, bf16[256,512]{1,0:T(8,128)(2,1)S(1)}, u32[]{:S(2)}, u32[]{:S(2)}) collective-permute-start(bf16[256,512]{1,0:T(8,128)(2,1)S(1)} %get-tuple-element.37), channel_id=1, source_target_pairs={{0,2},{2,4},{4,6},{6,0},{1,3},{3,5},{5,7},{7,1},{8,10},{10,12},{12... | collective-permute-start | bytes 786440 | tf_op jit(solution)/shard_map/ppermute | solution.py:171
  130.4 25.0 %all-to-all-start.2 = ((bf16[32,8,1024]{2,1,0:T(8,128)(2,1)}), bf16[32,8,1024]{2,1,0:T(8,128)(2,1)S(1)}, u32[]{:S(2)}, u32[]{:S(2)}) async-start(bf16[32,8,1024]{2,1,0:T(8,128)(2,1)} %bitcast.29), calls=%async_computation.2 | async-start | bytes 1048576 | tf_op jit(solution)/shard_map/all_to_all | solution.py:413
  140.9 19.8 %collective-permute-start.11 = (bf16[16,4096]{1,0:T(8,128)(2,1)S(1)}, bf16[16,4096]{1,0:T(8,128)(2,1)S(1)}, u32[]{:S(2)}, u32[]{:S(2)}) collective-permute-start(bf16[16,4096]{1,0:T(8,128)(2,1)S(1)} %get-tuple-element.42), channel_id=1, source_target_pairs={{0,2},{2,4},{4,6},{6,0},{1,3},{3,5},{5,7},{7,1},{8,10},{10,12},{12... | collective-permute-start | bytes 393224 | tf_op jit(solution)/shard_map/ppermute | solution.py:171
  141.2 19.5 %collective-permute-start.12 = (bf16[16,4096]{1,0:T(8,128)(2,1)S(1)}, bf16[16,4096]{1,0:T(8,128)(2,1)S(1)}, u32[]{:S(2)}, u32[]{:S(2)}) collective-permute-start(bf16[16,4096]{1,0:T(8,128)(2,1)S(1)} %get-tuple-element.44), channel_id=1, source_target_pairs={{0,4},{2,6},{4,0},{6,2},{1,5},{3,7},{5,1},{7,3},{8,12},{10,14},{12... | collective-permute-start | bytes 393224 | tf_op jit(solution)/shard_map/ppermute | solution.py:171
  144.7 15.9 %collective-permute-start.13 = (bf16[16,4096]{1,0:T(8,128)(2,1)S(1)}, bf16[16,4096]{1,0:T(8,128)(2,1)S(1)}, u32[]{:S(2)}, u32[]{:S(2)}) collective-permute-start(bf16[16,4096]{1,0:T(8,128)(2,1)S(1)} %get-tuple-element.43), channel_id=1, source_target_pairs={{0,6},{2,0},{4,2},{6,4},{1,7},{3,1},{5,3},{7,5},{8,14},{10,8},{12,... | collective-permute-start | bytes 393224 | tf_op jit(solution)/shard_map/ppermute | solution.py:171
  (30 other events, 191.8 us)

commit v3 on v2

--- a/solution.py
+++ b/solution.py
@@ -77,13 +77,13 @@
     def diagonal(i, unused):
         q_at = here * 128 + lax.broadcasted_iota(jnp.int32, (128, 512), 0)
         mask = lax.broadcasted_iota(jnp.int32, (128, 512), 1) < q_at
-        done = [tile(i * 4 + j, i * 4 + j, mask, jnp.zeros((128, 1), F32)) for j in range(4)]
-        for j in range(4):
-            acc_ref[i * 4 + j] = done[j][0]
-            carry_ref[i * 4 + j] = done[j][1]
+        done = [tile(j, j, mask, jnp.zeros((128, 1), F32)) for j in range(8)]
+        for j in range(8):
+            acc_ref[j] = done[j][0]
+            carry_ref[j] = done[j][1]
         return unused
 
-    lax.fori_loop(0, 2, diagonal, 0)
+    lax.fori_loop(0, 1, diagonal, 0)
 
     def sweep(i, unused):
         blocks = [steps_ref[i, 2 * j] for j in range(4)]

time: 167 us -> 167 us (level)
  no operation moved by 1% of the time
where the time goes in v3:
time: 167 us; the launch traced here: 166 us
  starting transfers between devices  64.4 us (39%)
  waiting for transfers between devices  50.9 us (30%)
  Pallas kernels  33.8 us (20%)
  local copies, waits for them, and re-layouts  11.2 us (7%)
  matrix products  2.93 us (2%)
  other arithmetic  2.06 us (1%)
    ppermute x30, starting transfers between devices, shifted(): lax.ppermute(value, axis, [(i, (i + by) % size) for i in range(size)])  46.8 us
    ppermute x30, waiting for transfers between devices, shifted(): lax.ppermute(value, axis, [(i, (i + by) % size) for i in range(size)])  26.1 us
    pallas_call x1, Pallas kernels, attend(): pl.pallas_call(attend_kernel, out_shape=jax.ShapeDtypeStruct((8, HEAD, 12...  14.8 us
    unnamed x43, local copies, waits for them, and re-layouts  10.3 us
    all_to_all x1, waiting for transfers between devices, experts(): lax.all_to_all(outgoing, ep, split_axis=0, concat_axis=0, tiled=True)  9.86 us
    all_to_all x1, starting transfers between devices, experts(): lax.all_to_all(result.reshape(Z * X, 8, width), ep, split_axis=0, concat_...  9.05 us
    all_to_all x1, waiting for transfers between devices, experts(): lax.all_to_all(result.reshape(Z * X, 8, width), ep, split_axis=0, concat_...  8.59 us
    all_to_all x1, waiting for transfers between devices, mixer(): attended = lax.all_to_all(out, 'z', split_axis=0, concat_axis=0, tiled=True)  6.34 us
  transfers between devices with their start and end apart: 33, of which 14 were waited for; matrix products, arithmetic and copies ran while one was open for 4% of the time, Pallas kernels for 18%

profile of v3, /device:TPU:2, one launch (start us, length us, event | category | flops | bytes accessed | tf_op | source)
XLA Modules:
  0.0 166.1 jit_solution(8289051648318397597)
XLA Ops:
  4.6 3.3 %collective-permute-start.1 = (bf16[208,128]{1,0:T(8,128)(2,1)}, bf16[208,128]{1,0:T(8,128)(2,1)S(1)}, u32[]{:S(2)}, u32[]{:S(2)}) collective-permute-start(bf16[208,128]{1,0:T(8,128)(2,1)} %get-tuple-element.24), channel_id=1, source_target_pairs={{0,64},{32,96},{64,128},{96,160},{128,192},{160,224},{192,0},{224,... | collective-permute-start | bytes 159752 | tf_op jit(solution)/shard_map/ppermute | solution.py:171
  7.8 4.0 %collective-permute-start.2 = (bf16[208,128]{1,0:T(8,128)(2,1)}, bf16[208,128]{1,0:T(8,128)(2,1)S(1)}, u32[]{:S(2)}, u32[]{:S(2)}) collective-permute-start(bf16[208,128]{1,0:T(8,128)(2,1)} %get-tuple-element.25), channel_id=1, source_target_pairs={{0,96},{32,128},{64,160},{96,192},{128,224},{160,0},{192,32},{224,... | collective-permute-start | bytes 159752 | tf_op jit(solution)/shard_map/ppermute | solution.py:171
  12.4 4.9 %collective-permute-start.4 = (bf16[208,128]{1,0:T(8,128)(2,1)}, bf16[208,128]{1,0:T(8,128)(2,1)S(1)}, u32[]{:S(2)}, u32[]{:S(2)}) collective-permute-start(bf16[208,128]{1,0:T(8,128)(2,1)} %get-tuple-element.27), channel_id=1, source_target_pairs={{0,160},{32,192},{64,224},{96,0},{128,32},{160,64},{192,96},{224,1... | collective-permute-start | bytes 159752 | tf_op jit(solution)/shard_map/ppermute | solution.py:171
  17.4 2.7 %collective-permute-start.5 = (bf16[208,128]{1,0:T(8,128)(2,1)}, bf16[208,128]{1,0:T(8,128)(2,1)S(1)}, u32[]{:S(2)}, u32[]{:S(2)}) collective-permute-start(bf16[208,128]{1,0:T(8,128)(2,1)} %get-tuple-element.28), channel_id=1, source_target_pairs={{0,192},{32,224},{64,0},{96,32},{128,64},{160,96},{192,128},{224,1... | collective-permute-start | bytes 159752 | tf_op jit(solution)/shard_map/ppermute | solution.py:171
  21.1 3.7 %collective-permute-done.4.refs_5_ = bf16[208,128]{1,0:T(8,128)(2,1)S(1)} collective-permute-done((bf16[208,128]{1,0:T(8,128)(2,1)}, bf16[208,128]{1,0:T(8,128)(2,1)S(1)}, u32[]{:S(2)}, u32[]{:S(2)}) %collective-permute-start.4) | collective-permute-done | bytes 53280 | tf_op jit(solution)/shard_map/ppermute | solution.py:171
  32.7 3.8 %shard_map.126 = (bf16[3072,128]{1,0:T(8,128)(2,1)}, bf16[3072,128]{1,0:T(8,128)(2,1)}, bf16[3072,128]{1,0:T(8,128)(2,1)}, bf16[3072,128]{1,0:T(8,128)(2,1)}) custom-call(bf16[4096,128]{1,0:T(8,128)(2,1)} %bitcast.36, bf16[4096,128]{1,0:T(8,128)(2,1)} %bitcast.37, bf16[128,4096]{1,0:T(8,128)(2,1)} %bitcast.38), custom_call_target="tpu_custom_call" | custom-call | tf_op jit(solution)/shard_map/pallas_call | solution.py:323
  38.2 2.9 %collective-permute-start.15 = (bf16[3072,128]{1,0:T(8,128)(2,1)}, bf16[3072,128]{1,0:T(8,128)(2,1)S(1)}, u32[]{:S(2)}, u32[]{:S(2)}) collective-permute-start(bf16[3072,128]{1,0:T(8,128)(2,1)} %get-tuple-element.32), channel_id=1, source_target_pairs={{0,4},{2,6},{4,0},{6,2},{1,5},{3,7},{5,1},{7,3},{8,12},{10,14},{12... | collective-permute-start | bytes 2359304 | tf_op jit(solution)/shard_map/ppermute | solution.py:171
  51.3 14.8 %shard_map.124 = bf16[8,64,128]{2,1,0:T(8,128)(2,1)} custom-call(bf16[208,128]{1,0:T(8,128)(2,1)S(1)} %copy-done.3, bf16[208,128]{1,0:T(8,128)(2,1)S(1)} %copy-done.5, bf16[208,128]{1,0:T(8,128)(2,1)S(1)} %copy-done.7, bf16[208,128]{1,0:T(8,128)(2,1)S(1)} %copy-done.9, bf16[208,128]{1,0:T(8,128)(2,1)S(1)} %copy-done.11, bf16[208,128]{1,0:T(8,128)(2,1)S(1)} %copy-done.13, ...), custom_call_target="tpu_custom_call" | custom-call | flops 4000000000 | bytes 2000000 | tf_op jit(solution)/shard_map/pallas_call | solution.py:109
  66.1 3.6 %all-to-all-start = ((bf16[8,64,128]{2,1,0:T(8,128)(2,1)}), bf16[8,64,128]{2,1,0:T(8,128)(2,1)S(1)}, u32[]{:S(2)}, u32[]{:S(2)}) async-start(bf16[8,64,128]{2,1,0:T(8,128)(2,1)} %shard_map.124), calls=%async_computation | async-start | bytes 262144 | tf_op jit(solution)/shard_map/all_to_all | solution.py:182
  69.7 2.7 %shard_map.125 = bf16[256,1024]{1,0:T(8,128)(2,1)} custom-call(s32[2,128]{1,0:T(2,128)} %bitcast.31, bf16[128,4096]{1,0:T(8,128)(2,1)} %rows_ref.1), custom_call_target="tpu_custom_call" | custom-call | tf_op jit(solution)/shard_map/pallas_call | solution.py:234
  72.4 6.3 %all-to-all-done = bf16[8,64,128]{2,1,0:T(8,128)(2,1)S(1)} async-done(((bf16[8,64,128]{2,1,0:T(8,128)(2,1)}), bf16[8,64,128]{2,1,0:T(8,128)(2,1)S(1)}, u32[]{:S(2)}, u32[]{:S(2)}) %all-to-all-start) | async-done | bytes 131104 | tf_op jit(solution)/shard_map/all_to_all | solution.py:182
  78.8 4.9 %all-to-all-start.1 = ((bf16[32,8,1024]{2,1,0:T(8,128)(2,1)}), bf16[32,8,1024]{2,1,0:T(8,128)(2,1)}, u32[]{:S(2)}, u32[]{:S(2)}) async-start(bf16[32,8,1024]{2,1,0:T(8,128)(2,1)} %bitcast.35), calls=%async_computation.1 | async-start | bytes 1048576 | tf_op jit(solution)/shard_map/all_to_all | solution.py:406
  84.8 2.9 %convolution_convert_fusion = bf16[128,4096]{1,0:T(8,128)(2,1)S(1)} fusion(bf16[512,128]{1,0:T(8,128)(2,1)S(1)} %bitcast.39, bf16[512,4096]{1,0:T(8,128)(2,1)} %param.15), kind=kOutput, calls=%fused_computation | convolution fusion | flops 537395200 | bytes 5373952 | tf_op jit(solution)/shard_map/dot_general | solution.py:184
  89.7 9.9 %all-to-all-done.1 = bf16[32,8,1024]{2,1,0:T(8,128)(2,1)} async-done(((bf16[32,8,1024]{2,1,0:T(8,128)(2,1)}), bf16[32,8,1024]{2,1,0:T(8,128)(2,1)}, u32[]{:S(2)}, u32[]{:S(2)}) %all-to-all-start.1) | async-done | bytes 524320 | tf_op jit(solution)/shard_map/all_to_all | solution.py:406
  99.6 3.3 %shard_map.127 = (f32[256,512]{1,0:T(8,128)S(1)}, bf16[256,512]{1,0:T(8,128)(2,1)S(1)}, bf16[256,512]{1,0:T(8,128)(2,1)S(1)}, bf16[256,512]{1,0:T(8,128)(2,1)S(1)}) custom-call(bf16[256,1024]{1,0:T(8,128)(2,1)} %bitcast.11.refs_0_, bf16[3072,128]{1,0:T(8,128)(2,1)S(1)} %copy-done, bf16[3072,128]{1,0:T(8,128)(2,1)S(1)} %collective-permute-done.14.refs_2_.refs_5_, ...), custom_call_target="tpu_custom_call" | custom-call | tf_op jit(solution)/shard_map/pallas_call | solution.py:345
  102.8 3.1 %collective-permute-start.21 = (bf16[256,512]{1,0:T(8,128)(2,1)S(1)}, bf16[256,512]{1,0:T(8,128)(2,1)S(1)}, u32[]{:S(2)}, u32[]{:S(2)}) collective-permute-start(bf16[256,512]{1,0:T(8,128)(2,1)S(1)} %get-tuple-element.35), channel_id=1, source_target_pairs={{0,6},{2,0},{4,2},{6,4},{1,7},{3,1},{5,3},{7,5},{8,14},{10,8},{12,... | collective-permute-start | bytes 786440 | tf_op jit(solution)/shard_map/ppermute | solution.py:171
  107.5 6.6 %collective-permute-done.21.p1_ref = bf16[256,512]{1,0:T(8,128)(2,1)S(1)} collective-permute-done((bf16[256,512]{1,0:T(8,128)(2,1)S(1)}, bf16[256,512]{1,0:T(8,128)(2,1)S(1)}, u32[]{:S(2)}, u32[]{:S(2)}) %collective-permute-start.21) | collective-permute-done | bytes 262176 | tf_op jit(solution)/shard_map/ppermute | solution.py:171
  115.2 2.7 %collective-permute-done.23.p3_ref = bf16[256,512]{1,0:T(8,128)(2,1)S(1)} collective-permute-done((bf16[256,512]{1,0:T(8,128)(2,1)S(1)}, bf16[256,512]{1,0:T(8,128)(2,1)S(1)}, u32[]{:S(2)}, u32[]{:S(2)}) %collective-permute-start.23) | collective-permute-done | bytes 262176 | tf_op jit(solution)/shard_map/ppermute | solution.py:171
  121.4 4.6 %collective-permute-done.24.refs_1_ = bf16[256,256]{1,0:T(8,128)(2,1)S(1)} collective-permute-done((bf16[256,256]{1,0:T(8,128)(2,1)S(1)}, bf16[256,256]{1,0:T(8,128)(2,1)S(1)}, u32[]{:S(2)}, u32[]{:S(2)}) %collective-permute-start.24) | collective-permute-done | bytes 131104 | tf_op jit(solution)/shard_map/ppermute | solution.py:171
  126.8 2.6 %shard_map.129 = bf16[256,1024]{1,0:T(8,128)(2,1)S(1)} custom-call(bf16[256,256]{1,0:T(8,128)(2,1)S(1)} %shard_map.128.refs_0_, bf16[256,256]{1,0:T(8,128)(2,1)S(1)} %collective-permute-done.24.refs_1_, bf16[256,256]{1,0:T(8,128)(2,1)S(1)} %collective-permute-done.25.refs_2_, bf16[256,256]{1,0:T(8,128)(2,1)} %collective-permute-done.26.refs_3_, ...), custom_call_target="tpu_custom_call" | custom-call | tf_op jit(solution)/shard_map/pallas_call | solution.py:389
  130.2 9.1 %all-to-all-start.2 = ((bf16[32,8,1024]{2,1,0:T(8,128)(2,1)}), bf16[32,8,1024]{2,1,0:T(8,128)(2,1)S(1)}, u32[]{:S(2)}, u32[]{:S(2)}) async-start(bf16[32,8,1024]{2,1,0:T(8,128)(2,1)} %bitcast.29), calls=%async_computation.2 | async-start | bytes 1048576 | tf_op jit(solution)/shard_map/all_to_all | solution.py:413
  140.9 3.6 %collective-permute-start.12 = (bf16[16,4096]{1,0:T(8,128)(2,1)S(1)}, bf16[16,4096]{1,0:T(8,128)(2,1)S(1)}, u32[]{:S(2)}, u32[]{:S(2)}) collective-permute-start(bf16[16,4096]{1,0:T(8,128)(2,1)S(1)} %get-tuple-element.44), channel_id=1, source_target_pairs={{0,4},{2,6},{4,0},{6,2},{1,5},{3,7},{5,1},{7,3},{8,12},{10,14},{12... | collective-permute-start | bytes 393224 | tf_op jit(solution)/shard_map/ppermute | solution.py:171
  146.5 8.6 %all-to-all-done.2 = bf16[32,8,1024]{2,1,0:T(8,128)(2,1)S(1)} async-done(((bf16[32,8,1024]{2,1,0:T(8,128)(2,1)}), bf16[32,8,1024]{2,1,0:T(8,128)(2,1)S(1)}, u32[]{:S(2)}, u32[]{:S(2)}) %all-to-all-start.2) | async-done | bytes 524320 | tf_op jit(solution)/shard_map/all_to_all | solution.py:413
  156.6 3.8 %collective-permute-start.28 = (bf16[2,16,1024]{2,1,0:T(8,128)(2,1)S(1)}, bf16[2,16,1024]{2,1,0:T(8,128)(2,1)S(1)}, u32[]{:S(2)}, u32[]{:S(2)}) collective-permute-start(bf16[2,16,1024]{2,1,0:T(8,128)(2,1)S(1)} %get-tuple-element.40), channel_id=1, source_target_pairs={{0,4},{2,6},{4,0},{6,2},{1,5},{3,7},{5,1},{7,3},{8,12},{10,14},{12... | collective-permute-start | bytes 196616 | tf_op jit(solution)/shard_map/ppermute | solution.py:171
  (101 shorter events, 46.9 us)
Async XLA Ops:
  2.6 14.7 %collective-permute-start = (bf16[208,128]{1,0:T(8,128)(2,1)}, bf16[208,128]{1,0:T(8,128)(2,1)S(1)}, u32[]{:S(2)}, u32[]{:S(2)}) collective-permute-start(bf16[208,128]{1,0:T(8,128)(2,1)} %get-tuple-element.23), channel_id=1, source_target_pairs={{0,32},{32,64},{64,96},{96,128},{128,160},{160,192},{192,224},{224... | collective-permute-start | bytes 159752 | tf_op jit(solution)/shard_map/ppermute | solution.py:171
  4.6 15.5 %collective-permute-start.1 = (bf16[208,128]{1,0:T(8,128)(2,1)}, bf16[208,128]{1,0:T(8,128)(2,1)S(1)}, u32[]{:S(2)}, u32[]{:S(2)}) collective-permute-start(bf16[208,128]{1,0:T(8,128)(2,1)} %get-tuple-element.24), channel_id=1, source_target_pairs={{0,64},{32,96},{64,128},{96,160},{128,192},{160,224},{192,0},{224,... | collective-permute-start | bytes 159752 | tf_op jit(solution)/shard_map/ppermute | solution.py:171
  7.8 13.2 %collective-permute-start.2 = (bf16[208,128]{1,0:T(8,128)(2,1)}, bf16[208,128]{1,0:T(8,128)(2,1)S(1)}, u32[]{:S(2)}, u32[]{:S(2)}) collective-permute-start(bf16[208,128]{1,0:T(8,128)(2,1)} %get-tuple-element.25), channel_id=1, source_target_pairs={{0,96},{32,128},{64,160},{96,192},{128,224},{160,0},{192,32},{224,... | collective-permute-start | bytes 159752 | tf_op jit(solution)/shard_map/ppermute | solution.py:171
  11.9 9.2 %collective-permute-start.3 = (bf16[208,128]{1,0:T(8,128)(2,1)}, bf16[208,128]{1,0:T(8,128)(2,1)S(1)}, u32[]{:S(2)}, u32[]{:S(2)}) collective-permute-start(bf16[208,128]{1,0:T(8,128)(2,1)} %get-tuple-element.26), channel_id=1, source_target_pairs={{0,128},{32,160},{64,192},{96,224},{128,0},{160,32},{192,64},{224,... | collective-permute-start | bytes 159752 | tf_op jit(solution)/shard_map/ppermute | solution.py:171
  12.4 12.3 %collective-permute-start.4 = (bf16[208,128]{1,0:T(8,128)(2,1)}, bf16[208,128]{1,0:T(8,128)(2,1)S(1)}, u32[]{:S(2)}, u32[]{:S(2)}) collective-permute-start(bf16[208,128]{1,0:T(8,128)(2,1)} %get-tuple-element.27), channel_id=1, source_target_pairs={{0,160},{32,192},{64,224},{96,0},{128,32},{160,64},{192,96},{224,1... | collective-permute-start | bytes 159752 | tf_op jit(solution)/shard_map/ppermute | solution.py:171
  27.9 13.2 %collective-permute-start.7 = (bf16[8,144,128]{2,1,0:T(8,128)(2,1)}, bf16[8,144,128]{2,1,0:T(8,128)(2,1)S(1)}, u32[]{:S(2)}, u32[]{:S(2)}) collective-permute-start(bf16[8,144,128]{2,1,0:T(8,128)(2,1)} %shard_map.123), channel_id=1, source_target_pairs={{0,8},{8,16},{16,24},{24,0},{1,9},{9,17},{17,25},{25,1},{2,10},{10... | collective-permute-start | bytes 884744 | tf_op jit(solution)/shard_map/ppermute | solution.py:171
  29.4 13.0 %collective-permute-start.8 = (bf16[8,144,128]{2,1,0:T(8,128)(2,1)}, bf16[8,144,128]{2,1,0:T(8,128)(2,1)}, u32[]{:S(2)}, u32[]{:S(2)}) collective-permute-start(bf16[8,144,128]{2,1,0:T(8,128)(2,1)} %shard_map.123), channel_id=1, source_target_pairs={{0,16},{8,24},{16,0},{24,8},{1,17},{9,25},{17,1},{25,9},{2,18},{10... | collective-permute-start | bytes 884744 | tf_op jit(solution)/shard_map/ppermute | solution.py:171
  30.5 14.3 %collective-permute-start.9 = (bf16[8,144,128]{2,1,0:T(8,128)(2,1)}, bf16[8,144,128]{2,1,0:T(8,128)(2,1)}, u32[]{:S(2)}, u32[]{:S(2)}) collective-permute-start(bf16[8,144,128]{2,1,0:T(8,128)(2,1)} %shard_map.123), channel_id=1, source_target_pairs={{0,24},{8,0},{16,8},{24,16},{1,25},{9,1},{17,9},{25,17},{2,26},{10... | collective-permute-start | bytes 884744 | tf_op jit(solution)/shard_map/ppermute | solution.py:171
  36.5 47.2 %collective-permute-start.14 = (bf16[3072,128]{1,0:T(8,128)(2,1)}, bf16[3072,128]{1,0:T(8,128)(2,1)S(1)}, u32[]{:S(2)}, u32[]{:S(2)}) collective-permute-start(bf16[3072,128]{1,0:T(8,128)(2,1)} %get-tuple-element.31), channel_id=1, source_target_pairs={{0,2},{2,4},{4,6},{6,0},{1,3},{3,5},{5,7},{7,1},{8,10},{10,12},{12... | collective-permute-start | bytes 2359304 | tf_op jit(solution)/shard_map/ppermute | solution.py:171
  38.2 46.1 %collective-permute-start.15 = (bf16[3072,128]{1,0:T(8,128)(2,1)}, bf16[3072,128]{1,0:T(8,128)(2,1)S(1)}, u32[]{:S(2)}, u32[]{:S(2)}) collective-permute-start(bf16[3072,128]{1,0:T(8,128)(2,1)} %get-tuple-element.32), channel_id=1, source_target_pairs={{0,4},{2,6},{4,0},{6,2},{1,5},{3,7},{5,1},{7,3},{8,12},{10,14},{12... | collective-permute-start | bytes 2359304 | tf_op jit(solution)/shard_map/ppermute | solution.py:171
  41.1 43.3 %collective-permute-start.16 = (bf16[3072,128]{1,0:T(8,128)(2,1)}, bf16[3072,128]{1,0:T(8,128)(2,1)S(1)}, u32[]{:S(2)}, u32[]{:S(2)}) collective-permute-start(bf16[3072,128]{1,0:T(8,128)(2,1)} %get-tuple-element.33), channel_id=1, source_target_pairs={{0,6},{2,0},{4,2},{6,4},{1,7},{3,1},{5,3},{7,5},{8,14},{10,8},{12,... | collective-permute-start | bytes 2359304 | tf_op jit(solution)/shard_map/ppermute | solution.py:171
  66.1 12.7 %all-to-all-start = ((bf16[8,64,128]{2,1,0:T(8,128)(2,1)}), bf16[8,64,128]{2,1,0:T(8,128)(2,1)S(1)}, u32[]{:S(2)}, u32[]{:S(2)}) async-start(bf16[8,64,128]{2,1,0:T(8,128)(2,1)} %shard_map.124), calls=%async_computation | async-start | bytes 262144 | tf_op jit(solution)/shard_map/all_to_all | solution.py:182
  78.8 20.8 %all-to-all-start.1 = ((bf16[32,8,1024]{2,1,0:T(8,128)(2,1)}), bf16[32,8,1024]{2,1,0:T(8,128)(2,1)}, u32[]{:S(2)}, u32[]{:S(2)}) async-start(bf16[32,8,1024]{2,1,0:T(8,128)(2,1)} %bitcast.35), calls=%async_computation.1 | async-start | bytes 1048576 | tf_op jit(solution)/shard_map/all_to_all | solution.py:406
  83.8 15.8 %collective-permute-start.18 = (bf16[3072,128]{1,0:T(8,128)(2,1)S(1)}, bf16[3072,128]{1,0:T(8,128)(2,1)}, u32[]{:S(2)}, u32[]{:S(2)}) collective-permute-start(bf16[3072,128]{1,0:T(8,128)(2,1)S(1)} %collective-permute-done.14.refs_2_.refs_5_), channel_id=1, source_target_pairs={{0,1},{1,0},{2,3},{3,2},{4,5},{5,4},{6,7},{7,6},{8,9},{9,8},{10,11... | collective-permute-start | bytes 2359304 | tf_op jit(solution)/shard_map/ppermute | solution.py:171
  84.3 15.3 %collective-permute-start.19 = (bf16[3072,128]{1,0:T(8,128)(2,1)S(1)}, bf16[3072,128]{1,0:T(8,128)(2,1)}, u32[]{:S(2)}, u32[]{:S(2)}) collective-permute-start(bf16[3072,128]{1,0:T(8,128)(2,1)S(1)} %collective-permute-done.15.refs_3_.refs_6_), channel_id=1, source_target_pairs={{0,1},{1,0},{2,3},{3,2},{4,5},{5,4},{6,7},{7,6},{8,9},{9,8},{10,11... | collective-permute-start | bytes 2359304 | tf_op jit(solution)/shard_map/ppermute | solution.py:171
  84.4 15.2 %collective-permute-start.20 = (bf16[3072,128]{1,0:T(8,128)(2,1)S(1)}, bf16[3072,128]{1,0:T(8,128)(2,1)}, u32[]{:S(2)}, u32[]{:S(2)}) collective-permute-start(bf16[3072,128]{1,0:T(8,128)(2,1)S(1)} %collective-permute-done.16.refs_4_.refs_7_), channel_id=1, source_target_pairs={{0,1},{1,0},{2,3},{3,2},{4,5},{5,4},{6,7},{7,6},{8,9},{9,8},{10,11... | collective-permute-start | bytes 2359304 | tf_op jit(solution)/shard_map/ppermute | solution.py:171
  89.6 49.6 %collective-permute-start.10 = (bf16[4,16,4096]{2,1,0:T(8,128)(2,1)}, bf16[4,16,4096]{2,1,0:T(8,128)(2,1)}, u32[]{:S(2)}, u32[]{:S(2)}) collective-permute-start(bf16[4,16,4096]{2,1,0:T(8,128)(2,1)} %dynamic-slice_bitcast_fusion), channel_id=1, source_target_pairs={{0,1},{1,0},{2,3},{3,2},{4,5},{5,4},{6,7},{7,6},{8,9},{9,8},{10,11... | collective-permute-start | bytes 1572872 | tf_op jit(solution)/shard_map/ppermute | solution.py:171
  102.8 11.3 %collective-permute-start.21 = (bf16[256,512]{1,0:T(8,128)(2,1)S(1)}, bf16[256,512]{1,0:T(8,128)(2,1)S(1)}, u32[]{:S(2)}, u32[]{:S(2)}) collective-permute-start(bf16[256,512]{1,0:T(8,128)(2,1)S(1)} %get-tuple-element.35), channel_id=1, source_target_pairs={{0,6},{2,0},{4,2},{6,4},{1,7},{3,1},{5,3},{7,5},{8,14},{10,8},{12,... | collective-permute-start | bytes 786440 | tf_op jit(solution)/shard_map/ppermute | solution.py:171
  105.9 9.3 %collective-permute-start.22 = (bf16[256,512]{1,0:T(8,128)(2,1)S(1)}, bf16[256,512]{1,0:T(8,128)(2,1)S(1)}, u32[]{:S(2)}, u32[]{:S(2)}) collective-permute-start(bf16[256,512]{1,0:T(8,128)(2,1)S(1)} %get-tuple-element.36), channel_id=1, source_target_pairs={{0,4},{2,6},{4,0},{6,2},{1,5},{3,7},{5,1},{7,3},{8,12},{10,14},{12... | collective-permute-start | bytes 786440 | tf_op jit(solution)/shard_map/ppermute | solution.py:171
  106.6 11.3 %collective-permute-start.23 = (bf16[256,512]{1,0:T(8,128)(2,1)S(1)}, bf16[256,512]{1,0:T(8,128)(2,1)S(1)}, u32[]{:S(2)}, u32[]{:S(2)}) collective-permute-start(bf16[256,512]{1,0:T(8,128)(2,1)S(1)} %get-tuple-element.37), channel_id=1, source_target_pairs={{0,2},{2,4},{4,6},{6,0},{1,3},{3,5},{5,7},{7,1},{8,10},{10,12},{12... | collective-permute-start | bytes 786440 | tf_op jit(solution)/shard_map/ppermute | solution.py:171
  130.2 25.0 %all-to-all-start.2 = ((bf16[32,8,1024]{2,1,0:T(8,128)(2,1)}), bf16[32,8,1024]{2,1,0:T(8,128)(2,1)S(1)}, u32[]{:S(2)}, u32[]{:S(2)}) async-start(bf16[32,8,1024]{2,1,0:T(8,128)(2,1)} %bitcast.29), calls=%async_computation.2 | async-start | bytes 1048576 | tf_op jit(solution)/shard_map/all_to_all | solution.py:413
  140.6 19.8 %collective-permute-start.11 = (bf16[16,4096]{1,0:T(8,128)(2,1)S(1)}, bf16[16,4096]{1,0:T(8,128)(2,1)S(1)}, u32[]{:S(2)}, u32[]{:S(2)}) collective-permute-start(bf16[16,4096]{1,0:T(8,128)(2,1)S(1)} %get-tuple-element.42), channel_id=1, source_target_pairs={{0,2},{2,4},{4,6},{6,0},{1,3},{3,5},{5,7},{7,1},{8,10},{10,12},{12... | collective-permute-start | bytes 393224 | tf_op jit(solution)/shard_map/ppermute | solution.py:171
  140.9 19.5 %collective-permute-start.12 = (bf16[16,4096]{1,0:T(8,128)(2,1)S(1)}, bf16[16,4096]{1,0:T(8,128)(2,1)S(1)}, u32[]{:S(2)}, u32[]{:S(2)}) collective-permute-start(bf16[16,4096]{1,0:T(8,128)(2,1)S(1)} %get-tuple-element.44), channel_id=1, source_target_pairs={{0,4},{2,6},{4,0},{6,2},{1,5},{3,7},{5,1},{7,3},{8,12},{10,14},{12... | collective-permute-start | bytes 393224 | tf_op jit(solution)/shard_map/ppermute | solution.py:171
  144.5 15.9 %collective-permute-start.13 = (bf16[16,4096]{1,0:T(8,128)(2,1)S(1)}, bf16[16,4096]{1,0:T(8,128)(2,1)S(1)}, u32[]{:S(2)}, u32[]{:S(2)}) collective-permute-start(bf16[16,4096]{1,0:T(8,128)(2,1)S(1)} %get-tuple-element.43), channel_id=1, source_target_pairs={{0,6},{2,0},{4,2},{6,4},{1,7},{3,1},{5,3},{7,5},{8,14},{10,8},{12,... | collective-permute-start | bytes 393224 | tf_op jit(solution)/shard_map/ppermute | solution.py:171
  (30 other events, 191.5 us)
